TPU v7x, 256 devices: a 4x2x16 block of a 4x16x16 slice. The times are simulated.
256 devices in a mesh: grp: 2 (over y), sp: 16 (over z), tp: 8 (over x, core).
Axes of the slice: x: 4, y: 2, z: 16, core: 2. Of those that a mesh axis runs over, the one named last changes fastest.
The devices are a block of a 4x16x16 slice.
Arguments:
- tokens: bfloat16 [16384, 4096], P(('grp', 'sp', 'tp')), parts along dimension 0, may hold values from -6 to 6
- norm_gain: float32 [4096], replicated, may hold values from 0.1 to 1.9
- query_diff: bfloat16 [4096, 2048], P('sp', 'tp'), may hold values from -1.25 to 1.25
- key_diff: bfloat16 [4096, 2048], P('sp', 'tp'), may hold values from -1.25 to 1.25
- value_diff: bfloat16 [4096, 2048], P('sp', 'tp'), may hold values from -0.09375 to 0.09375
- lam: float32 [8], P('tp'), may hold values from 0.3 to 0.8
- output_norm_gain: float32 [256], replicated, may hold values from 0.1 to 1.9
- query_win: bfloat16 [4096, 2048], P('sp', 'tp'), may hold values from -1.25 to 1.25
- keyval_win: bfloat16 [4, 4096, 256], P(None, 'sp'), may hold values from -1.25 to 1.25
- sink: float32 [16], P('tp'), may hold values from 4 to 7
- proj_diff: bfloat16 [2048, 4096], P('tp'), may hold values from -0.125 to 0.125
- proj_win: bfloat16 [2048, 4096], P('tp'), may hold values from -0.79296875 to 0.79296875
Outputs:
- mixed: bfloat16 [16384, 4096], P(('grp', 'sp', 'tp')), parts along dimension 0
There are 2 independent parts, one for each index of `grp`. A program takes and returns all parts, laid end to end along the dimension named above; an argument that names none is the same for every part. Nothing has to cross between parts.
All inputs are finite; a program needn't handle non-finite values.
Results may differ from a plain program's by a relative error of at most 0.015.
Values may be sent and summed in bfloat16 or wider, within the bound.
A program may use at most 128 MiB of HBM per device.

v0:
```python
import math

import jax
import jax.numpy as jnp
from jax import lax
from jax.sharding import Mesh
from jax.sharding import PartitionSpec as P

HEAD = 128
WIN_HEADS = 16
KV_HEADS = 4
WINDOW = 128
VDIM = 256
TP = ("tp_0", "tp_1")
GRP_SP_TP = ("grp", "sp", "tp_0", "tp_1")


EPS = 1e-06


def in_order(parts, dim):
    shape = list(parts.shape[1:])
    shape[dim] *= parts.shape[0]
    return jnp.moveaxis(parts, 0, dim).reshape(shape)


def stacked_from(x, axes, order):
    parts = x[None]
    for k in order:
        parts = lax.all_gather(parts, axes[k], axis=0, tiled=True)
    block = [lax.axis_size(axes[k]) for k in reversed(order)]
    parts = parts.reshape(*block, *x.shape)
    turned = sorted(range(len(order)), key=lambda place: order[len(order) - 1 - place])
    return parts.transpose(*turned, *range(len(order), parts.ndim)).reshape(-1, *x.shape)


def gathered_by_axis(x, axes, order, dim):
    return in_order(stacked_from(x, axes, order), dim)


def side_by_side(arrays, axis, dim, along):
    both = jnp.concatenate(arrays, axis=along)
    out, at, done = (lax.all_gather(both, axis, axis=dim, tiled=True), 0, [])
    for a in arrays:
        done.append(lax.slice_in_dim(out, at, at + a.shape[along], axis=along))
        at += a.shape[along]
    return tuple(done)


def padded_2(x, sides, width):
    for axis, dim in sides:
        devices, length = (lax.axis_size(axis), x.shape[dim])
        up = [(i, (i + 1) % devices) for i in range(devices - 1)]
        down = [(j, i) for i, j in up]
        last = lax.slice_in_dim(x, length - width, length, axis=dim)
        first = lax.slice_in_dim(x, 0, width, axis=dim)
        before = lax.ppermute(last, axis, up)
        after = lax.ppermute(first, axis, down)
        x = jnp.concatenate([before, x, after], axis=dim)
    return x


def root_mean_square_rows(values, gain):
    return values * lax.rsqrt(jnp.mean(values * values, axis=-1, keepdims=True) + EPS) * gain


def body(
    tokens,
    norm_gain,
    query_diff,
    key_diff,
    value_diff,
    lam,
    output_norm_gain,
    query_win,
    keyval_win,
    sink,
    proj_diff,
    proj_win,
):
    normed = root_mean_square_rows(tokens.astype(jnp.float32), norm_gain).astype(jnp.bfloat16)
    heads_diff = lam.shape[0]
    heads_win = sink.shape[0]
    group = WIN_HEADS // KV_HEADS
    kv_index = lax.axis_index(TP) * heads_win // group
    kv_local = lax.dynamic_index_in_dim(keyval_win, kv_index, 0, keepdims=False)
    pieces = [query_diff, key_diff, value_diff, query_win, kv_local]
    stacked = jnp.concatenate(pieces, axis=1)
    rows_all = gathered_by_axis(normed, TP, (0, 1), 0)
    projected = jnp.dot(
        rows_all,
        lax.all_gather(stacked, "sp", axis=0, tiled=True),
        preferred_element_type=jnp.float32,
    )
    projected = projected.astype(jnp.bfloat16)
    output_list = []
    offset = 0
    for piece in pieces:
        output_list.append(projected[:, offset : offset + piece.shape[1]])
        offset = offset + piece.shape[1]
    q_diff, k_diff, v_diff, q_win, kv_win = output_list
    tok = projected.shape[0]
    scale = HEAD ** (-0.5)
    q_four = q_diff.reshape(tok, heads_diff, 2, HEAD)
    start_state = (
        jnp.full((heads_diff, 2, tok), -jnp.inf, jnp.float32),
        jnp.zeros((heads_diff, 2, tok), jnp.float32),
        jnp.zeros((heads_diff, 2, tok, VDIM), jnp.float32),
    )
    carry = start_state
    keys, values = side_by_side((k_diff, v_diff), "sp", 0, 1)
    rows = keys.shape[0]
    step = math.gcd(rows, 1024)
    key_blocks = keys.reshape(rows // step, step, heads_diff, 2, HEAD)
    value_blocks = values.reshape(rows // step, step, heads_diff, VDIM)

    def one(state, block):
        top, total, acc = state
        key_part, value_part = block
        scores = (
            jnp.einsum("qhmd,khmd->hmqk", q_four, key_part, preferred_element_type=jnp.float32)
            * scale
        )
        new_top = jnp.maximum(top, jnp.max(scores, axis=-1))
        expo = jnp.exp(scores - new_top[..., None])
        fade = jnp.exp(top - new_top)
        total = total * fade + jnp.sum(expo, axis=-1)
        acc = acc * fade[..., None] + jnp.einsum(
            "hmqk,khe->hmqe",
            expo.astype(jnp.bfloat16),
            value_part,
            preferred_element_type=jnp.float32,
        )
        return ((new_top, total, acc), None)

    carry, unused = lax.scan(one, carry, (key_blocks, value_blocks))
    top, total, acc = carry
    attention_maps = acc / total[..., None]
    difference_output = attention_maps[:, 0] - lam[:, None, None] * attention_maps[:, 1]
    differential_output = root_mean_square_rows(difference_output, output_norm_gain).astype(
        jnp.bfloat16
    )
    differential_output = jnp.transpose(differential_output, (1, 0, 2)).reshape(
        tok, heads_diff * VDIM
    )
    padded = padded_2(kv_win, (("sp", 0),), WINDOW)
    nblocks = tok // WINDOW
    blocks = padded.reshape(nblocks + 2, WINDOW, 2 * HEAD)
    band = jnp.concatenate([blocks[:-2], blocks[1:-1], blocks[2:]], axis=1)
    q_blocks = q_win.reshape(nblocks, WINDOW, heads_win, HEAD)
    scores = (
        jnp.einsum("nqhd,nkd->nhqk", q_blocks, band[..., :HEAD], preferred_element_type=jnp.float32)
        * scale
    )
    q_index = jnp.arange(WINDOW)
    k_index = jnp.arange(3 * WINDOW)
    relative = k_index[None, :] - WINDOW - q_index[:, None]
    first_key = lax.axis_index("sp") * tok - WINDOW
    key_pos = first_key + jnp.arange(nblocks)[:, None] * WINDOW + k_index[None, :]
    inside = (key_pos >= 0) & (key_pos < tok * lax.axis_size("sp"))
    valid = (jnp.abs(relative) <= WINDOW)[None] & inside[:, None, :]
    scores = jnp.where(valid[:, None], scores, -jnp.inf)
    sink_logit = sink[None, :, None, None]
    top_win = jnp.maximum(jnp.max(scores, axis=-1, keepdims=True), sink_logit)
    expo = jnp.exp(scores - top_win)
    weights = expo / (jnp.sum(expo, axis=-1, keepdims=True) + jnp.exp(sink_logit - top_win))
    y_win = jnp.einsum(
        "nhqk,nkd->nqhd",
        weights.astype(jnp.bfloat16),
        band[..., HEAD:],
        preferred_element_type=jnp.float32,
    ).astype(jnp.bfloat16)
    y_win = y_win.reshape(tok, heads_win * HEAD)
    summed = jnp.dot(differential_output, proj_diff, preferred_element_type=jnp.float32)
    return lax.psum_scatter(
        (summed + jnp.dot(y_win, proj_win, preferred_element_type=jnp.float32)).astype(
            jnp.bfloat16
        ),
        TP,
        scatter_dimension=0,
        tiled=True,
    )


def solution(mesh):
    torus = Mesh(
        mesh.devices.reshape(mesh.shape["grp"], mesh.shape["sp"], 4, 2),
        ("grp", "sp", "tp_0", "tp_1"),
    )
    return jax.shard_map(
        body,
        mesh=torus,
        in_specs=(
            P(GRP_SP_TP, None),
            P(),
            P("sp", TP),
            P("sp", TP),
            P("sp", TP),
            P(TP),
            P(),
            P("sp", TP),
            P(None, "sp", None),
            P(TP),
            P(TP, None),
            P(TP, None),
        ),
        out_specs=P(GRP_SP_TP, None),
        check_vma=False,
    )
```

profile of v0, /device:TPU:33, one launch (start us, length us, event | category | flops | bytes accessed | tf_op | source)
XLA Modules:
  0.0 441.2 jit_solution(13832787000681153917)
XLA Ops:
  8.0 2.0 fusion.24
  10.2 51.3 %all-gather.12.cloned.1.call-done = bf16[256,4096]{1,0:T(8,128)(2,1)} async-done(((bf16[64,4096]{1,0:T(8,128)(2,1)}), bf16[256,4096]{1,0:T(8,128)(2,1)}) %all-gather.12.cloned.1.call-update) | async-done | bytes 2097168 | tf_op jit(solution)/shard_map/all_gather | solution.py:30
  63.7 23.6 %all-gather.6.cloned.1.call-done = bf16[8,64,4096]{2,1,0:T(8,128)(2,1)} async-done(((bf16[4,64,4096]{2,1,0:T(8,128)(2,1)}), bf16[8,64,4096]{2,1,0:T(8,128)(2,1)}) %all-gather.6.cloned.1.call-update) | async-done | bytes 4194320 | tf_op jit(solution)/shard_map/all_gather | solution.py:30
  87.3 4.7 %copy.38 = bf16[4,2,64,4096]{3,2,1,0:T(8,128)(2,1)} copy(bf16[4,2,64,4096]{3,2,0,1:T(8,128)(2,1)} %bitcast.110) | data formatting | bytes 8388608 | tf_op jit(solution)/shard_map/transpose | solution.py:34
  92.0 122.2 %all-gather.8.cloned.1.call-done = bf16[4096,1280]{1,0:T(8,128)(2,1)} async-done(((bf16[256,1280]{1,0:T(8,128)(2,1)}), bf16[4096,1280]{1,0:T(8,128)(2,1)}) %all-gather.8.cloned.1.call-update) | async-done | bytes 10485776 | tf_op jit(solution)/shard_map/all_gather | solution.py:92
  214.2 10.4 %convolution_convert_fusion = bf16[512,1280]{1,0:T(8,128)(2,1)S(1)} fusion(bf16[512,4096]{1,0:T(8,128)(2,1)} %bitcast.111, bf16[4096,1280]{1,0:T(8,128)(2,1)} %all-gather.8.cloned.1.call-done), kind=kOutput, calls=%fused_computation.26 | convolution fusion | flops 5369364480 | bytes 15990784 | tf_op jit(solution)/shard_map/dot_general | solution.py:90
  228.2 1.4 collective-permute-start
  229.6 1.5 collective-permute-start.1
  232.5 2.3 collective-permute-done.1
  236.4 91.4 %all-gather.10.cloned.1.call-done = bf16[8192,512]{1,0:T(8,128)(2,1)} async-done(((bf16[512,512]{1,0:T(8,128)(2,1)}), bf16[8192,512]{1,0:T(8,128)(2,1)}) %all-gather.10.cloned.1.call-update) | async-done | bytes 8388624 | tf_op jit(solution)/shard_map/all_gather | solution.py:43
  327.9 5.7 %fusion.39 = (bf16[8192,256]{1,0:T(8,128)(2,1)}, bf16[8192,256]{1,0:T(8,128)(2,1)}) fusion(bf16[8192,512]{1,0:T(8,128)(2,1)} %all-gather.10.cloned.1.call-done), kind=kLoop, calls=%fused_computation.73 | loop fusion | bytes 16777216 | tf_op jit(solution)/shard_map/slice | solution.py:45
  333.6 6.9 %reshape.210 = bf16[8,1024,1,2,128]{4,3,1,0,2:T(2,128)(2,1)} reshape(bf16[8192,256]{1,0:T(8,128)(2,1)} %get-tuple-element.116) | data formatting | bytes 8388608 | tf_op jit(solution)/shard_map/reshape | solution.py:114
  340.5 47.5 %while.15 = (s32[]{:T(128)}, f32[1,2,512]{2,1,0:T(2,128)S(1)}, f32[1,2,512]{2,1,0:T(2,128)S(1)}, f32[1,2,512,256]{3,2,1,0:T(8,128)}, bf16[8,1024,1,2,128]{4,3,1,...) while((s32[]{:T(128)}, f32[1,2,512]{2,1,0:T(2,128)S(1)}, ...), condition=%wide.region_4.5_spmd.clone, body=%wide.region_1.4_spmd.clone.sunk | while | flops 814487552 | bytes 25493680 | solution.py:136
  343.4 2.1 fusion.56
  349.3 2.1 fusion.56
  355.3 2.1 fusion.56
  361.2 2.1 fusion.56
  367.2 2.1 fusion.56
  373.1 2.1 fusion.56
  379.0 2.1 fusion.56
  385.0 2.1 fusion.56
  388.0 1.4 broadcast_divide_fusion
  391.3 3.3 add_convert_fusion
  394.6 40.1 %reduce-scatter.2.cloned.1.call-done = bf16[64,4096]{1,0:T(8,128)(2,1)} async-done(((bf16[512,4096]{1,0:T(8,128)(2,1)}), bf16[64,4096]{1,0:T(8,128)(2,1)}) %reduce-scatter.2.cloned.1.call-update) | async-done | bytes 524304 | tf_op jit(solution)/shard_map/reduce_scatter | solution.py:175
  (145 shorter events, 41.7 us)
Async XLA Ops:
  6.5 383.1 %copy-start = (bf16[256,4096]{1,0:T(8,128)(2,1)S(1)}, bf16[256,4096]{1,0:T(8,128)(2,1)}, u32[]{:S(2)}) copy-start(bf16[256,4096]{1,0:T(8,128)(2,1)} %param.24) | copy-start | bytes 6291460
  6.6 55.2 %copy-start.7 = (bf16[256,256]{1,0:T(8,128)(2,1)S(1)}, bf16[256,256]{1,0:T(8,128)(2,1)}, u32[]{:S(2)}) copy-start(bf16[256,256]{1,0:T(8,128)(2,1)} %param.16) | copy-start | bytes 393220
  6.6 55.2 %copy-start.8 = (bf16[256,256]{1,0:T(8,128)(2,1)S(1)}, bf16[256,256]{1,0:T(8,128)(2,1)}, u32[]{:S(2)}) copy-start(bf16[256,256]{1,0:T(8,128)(2,1)} %param.17) | copy-start | bytes 393220
  6.6 55.2 %copy-start.9 = (bf16[256,256]{1,0:T(8,128)(2,1)S(1)}, bf16[256,256]{1,0:T(8,128)(2,1)}, u32[]{:S(2)}) copy-start(bf16[256,256]{1,0:T(8,128)(2,1)} %param.18) | copy-start | bytes 393220
  6.6 55.2 %copy-start.10 = (bf16[256,256]{1,0:T(8,128)(2,1)S(1)}, bf16[256,256]{1,0:T(8,128)(2,1)}, u32[]{:S(2)}) copy-start(bf16[256,256]{1,0:T(8,128)(2,1)} %param.21) | copy-start | bytes 393220
  6.6 55.0 %all-gather.12.cloned.1.call-start = ((), (), s32[]{:S(2)}) async-start(), calls=%async_computation.5 | async-start | bytes 2621440 | tf_op jit(solution)/shard_map/all_gather | solution.py:30
  10.1 77.2 %all-gather.6.cloned.1.call-start = ((), (), s32[]{:S(2)}) async-start(), calls=%async_computation.1 | async-start | bytes 6291456 | tf_op jit(solution)/shard_map/all_gather | solution.py:30
  61.6 152.6 %all-gather.8.cloned.1.call-start = ((), (), s32[]{:S(2)}) async-start(), calls=%async_computation.2 | async-start | bytes 11141120 | tf_op jit(solution)/shard_map/all_gather | solution.py:92
  63.6 264.2 %all-gather.10.cloned.1.call-start = ((), (), s32[]{:S(2)}) async-start(), calls=%async_computation.3 | async-start | bytes 8912896 | tf_op jit(solution)/shard_map/all_gather | solution.py:43
  224.6 5.0 %copy-start.2 = (bf16[512,1280]{1,0:T(8,128)(2,1)}, bf16[512,1280]{1,0:T(8,128)(2,1)S(1)}, u32[]{:S(2)}) copy-start(bf16[512,1280]{1,0:T(8,128)(2,1)S(1)} %convolution_convert_fusion) | copy-start | bytes 3932164
  225.6 209.1 %reduce-scatter.2.cloned.1.call-start = ((), (), s32[]{:S(2)}) async-start(), calls=%async_computation.4 | async-start | bytes 4718592 | tf_op jit(solution)/shard_map/reduce_scatter | solution.py:175
  228.2 7.2 %copy-start.12 = (f32[2]{0:T(128)S(1)}, f32[2]{0:T(128)}, u32[]{:S(2)}) copy-start(f32[2]{0:T(128)} %param.23) | copy-start | bytes 28
  228.2 4.4 collective-permute-start
  229.6 5.3 %collective-permute-start.1 = (bf16[128,256]{1,0:T(8,128)(2,1)}, bf16[128,256]{1,0:T(8,128)(2,1)S(1)}, u32[]{:S(2)}, u32[]{:S(2)}) collective-permute-start(bf16[128,256]{1,0:T(8,128)(2,1)} %get-tuple-element.121), channel_id=1, source_target_pairs={{8,0},{16,8},{24,16},{32,24},{40,32},{48,40},{56,48},{64,56},{72,6... | collective-permute-start | bytes 196616 | tf_op jit(solution)/shard_map/ppermute | solution.py:58
  231.1 3.9 copy-start.6
  340.5 49.1 %copy-start.11 = (f32[256]{0:T(256)S(1)}, f32[256]{0:T(256)}, u32[]{:S(2)}) copy-start(f32[256]{0:T(256)} %param.20) | copy-start | bytes 3076
  341.9 1.5 copy-start.3
  347.9 1.5 copy-start.3
  353.8 1.5 copy-start.3
  359.8 1.5 copy-start.3
  365.7 1.5 copy-start.3
  371.6 1.5 copy-start.3
  377.6 1.5 copy-start.3
  389.7 1.6 copy-start.1
  (10 other events, 10.2 us)
Sparse Core Ops, SparseCore 0:
  10.3 51.2 all-gather.11
  63.4 23.8 all-gather.5
  89.1 125.0 all-gather.7
  225.7 102.1 all-gather.9
  394.7 39.9 reduce-scatter.1
where the time goes:
time: 443 us; the launch traced here: 441 us
  waiting for transfers between devices  331 us (75%)
  local copies, waits for them, and re-layouts  41.4 us (9%)
  matrix products  38.1 us (9%)
  between operations  14.2 us (3%)
  other arithmetic  12.5 us (3%)
    all_gather x1, waiting for transfers between devices, body(): lax.all_gather(stacked, 'sp', axis=0, tiled=True)  122 us
    all_gather x1, waiting for transfers between devices, side_by_side(): out, at, done = (lax.all_gather(both, axis, axis=dim, tiled=True), 0, [])  91.4 us
    all_gather x2, waiting for transfers between devices, stacked_from(): parts = lax.all_gather(parts, axes[k], axis=0, tiled=True)  74.9 us
    reduce_scatter x1, waiting for transfers between devices, body(): lax.psum_scatter((summed + jnp.dot(y_win, proj_win, preferred_element_typ...  40.1 us
    dot_general x8, matrix products, one(): jnp.einsum('hmqk,khe->hmqe', expo.astype(jnp.bfloat16), value_part, prefe...  16.5 us
    dynamic_slice x8, local copies, waits for them, and re-layouts, body(): carry, unused = lax.scan(one, carry, (key_blocks, value_blocks))  11.2 us
    dot_general x1, matrix products, body(): jnp.dot(rows_all, lax.all_gather(stacked, 'sp', axis=0, tiled=True), pref...  10.4 us
  transfers between devices with their start and end apart: 7, of which 6 were waited for; matrix products, arithmetic and copies ran while one was open for 2% of the time, Pallas kernels for 0%

commit v1 on v0

v1 whole, which is shorter than its diff:
```python
import functools

import jax
import jax.numpy as jnp
from jax import lax
from jax.experimental import pallas as pl
from jax.experimental.pallas import tpu as pltpu
from jax.sharding import Mesh
from jax.sharding import PartitionSpec as P

HEAD = 128
WIN_HEADS = 16
KV_HEADS = 4
WINDOW = 128
VDIM = 256
NX = 4
TP = ("tp_0", "tp_1")
GRP_SP_TP = ("grp", "sp", "tp_0", "tp_1")
EPS = 1e-06
LOG2E = 1.4426950408889634
BF16 = jnp.bfloat16
F32 = jnp.float32
MESH = pl.DeviceIdType.MESH
DMA = pltpu.SemaphoreType.DMA
VMEM = pltpu.VMEM
ANY = pl.ANY


def remote(src, dst, send_sem, recv_sem, where):
    return pltpu.make_async_remote_copy(
        src_ref=src,
        dst_ref=dst,
        send_sem=send_sem,
        recv_sem=recv_sem,
        device_id=where,
        device_id_type=MESH,
    )


def greet(peers):
    barrier = pltpu.get_barrier_semaphore()
    for peer in peers:
        pl.semaphore_signal(barrier, inc=1, device_id=peer, device_id_type=MESH)
    pl.semaphore_wait(barrier, len(peers))


class Ring:
    def __init__(self, n, buf, half, send, recv):
        self.n, self.buf, self.half, self.send, self.recv = n, buf, half, send, recv
        self.me = lax.axis_index("sp")
        self.to = (
            {"sp": lax.rem(self.me + 1, n)},
            {"sp": lax.rem(self.me + n - 1, n)},
        )

    def origin(self, d, s):
        return lax.rem(self.me + (self.n - s if d == 0 else s), self.n)

    def piece(self, d, s, k, hops):
        b = k if d == 0 else 1 - k
        ref = self.buf.at[self.origin(d, hops), pl.ds(b * self.half, self.half)]
        return remote(ref, ref, self.send.at[d, s, k], self.recv.at[d, s, k], self.to[d])

    def start(self, s, k):
        for d in (0, 1):
            self.piece(d, s, k, s).start()

    def land(self, s, k):
        for d in (0, 1):
            self.piece(d, s, k, s + 1).wait_recv()

    def drain(self):
        last = self.n // 2 - 1

        def one(s, carry):
            for k in (0, 1):
                for d in (0, 1):
                    self.piece(d, s, k, s).wait_send()
            return carry

        lax.fori_loop(0, last, one, 0)
        for d in (0, 1):
            self.piece(d, last, 0, last).wait_send()


class Side:
    def __init__(self, own, slots, half, xs, xr, cs, cr):
        self.own, self.slots, self.half = own, slots, half
        self.xs, self.xr, self.cs, self.cr = xs, xr, cs, cr
        self.x = lax.axis_index("tp_0")
        self.c = lax.axis_index("tp_1")
        self.to = (
            {"tp_0": lax.rem(self.x + 1, NX)},
            {"tp_0": lax.rem(self.x + NX - 1, NX)},
        )
        self.other = {"tp_1": 1 - self.c}

    def spot(self, rel, h, core):
        slot = 2 * lax.rem(self.x + rel, NX) + core
        return self.slots.at[slot, pl.ds(h * self.half, self.half)]

    def source(self, rel, h):
        if rel == 0 and self.own is not None:
            return self.own.at[pl.ds(h * self.half, self.half)]
        return self.spot(rel, h, self.c)

    def half_of(self, d, k):
        return (0, 1, 0)[k] if d == 0 else (1, 0, 1)[k]

    def out(self, d, k):
        rel = 0 if k < 2 else (3 if d == 0 else 1)
        h = self.half_of(d, k)
        return remote(
            self.source(rel, h), self.spot(rel, h, self.c), self.xs.at[d, k], self.xr.at[d, k], self.to[d]
        )

    def inward(self, d, k):
        rel = (3 if d == 0 else 1) if k < 2 else 2
        h = self.half_of(d, k)
        ref = self.spot(rel, h, self.c)
        return rel, h, remote(ref, ref, self.xs.at[d, k], self.xr.at[d, k], self.to[d])

    def across(self, rel, h):
        return remote(
            self.source(rel, h), self.spot(rel, h, self.c), self.cs.at[rel, h], self.cr.at[rel, h], self.other
        )

    def start(self):
        for k in (0, 1):
            for d in (0, 1):
                self.out(d, k).start()
        for h in (0, 1):
            self.across(0, h).start()

    def step(self, k):
        for d in (0, 1):
            rel, h, copy = self.inward(d, k)
            copy.wait_recv()
            if k == 0:
                self.out(d, 2).start()
            self.across(rel, h).start()

    def finish(self):
        for rel in range(NX):
            for h in (0, 1):
                ref = self.spot(rel, h, 1 - self.c)
                remote(ref, ref, self.cs.at[rel, h], self.cr.at[rel, h], self.other).wait_recv()

    def drain(self):
        for k in (0, 1, 2):
            for d in (0, 1):
                self.out(d, k).wait_send()
        for rel in range(NX):
            for h in (0, 1):
                self.across(rel, h).wait_send()


def side_sems():
    return [DMA((2, 3)), DMA((2, 3)), DMA((NX, 2)), DMA((NX, 2))]


def project_kernel(
    n, heads_win, tok, gain, kd, vd, qd, qw, kvw, pw,
    kv_out, q_out, qw_out, kvw_out, pw_out,
    wbuf, raw, nbuf, acc, hold, lsem, zs, zr, *sems,
):
    me, x, c = (lax.axis_index(a) for a in ("sp", "tp_0", "tp_1"))
    t = 2 * x + c
    group = WIN_HEADS // KV_HEADS
    local = []
    at = 0
    for w in (kd, vd, qd, qw):
        width = w.shape[1]
        local.append((w, wbuf.at[me, :, pl.ds(at, width)]))
        at += width
    part = kvw.shape[2] // 2
    local.append(
        (
            kvw.at[t * heads_win // group, :, pl.ds(pl.multiple_of(c * part, part), part)],
            wbuf.at[me, :, pl.ds(at, part)],
        )
    )
    local.append((tok, raw.at[t]))
    local.append((pw, hold))
    local = [pltpu.make_async_copy(a, b, lsem.at[i]) for i, (a, b) in enumerate(local)]
    for copy in local:
        copy.start()
    keep = pltpu.make_async_copy(hold, pw_out.at[t], lsem.at[len(local)])

    ring = Ring(n, wbuf, wbuf.shape[1] // 2, zs, zr)
    rows = raw.shape[1]
    side = Side(None, raw, rows // 2, *sems[:4])
    late = Side(pw, pw_out, pw.shape[0] // 2, *sems[4:])
    greet([ring.to[0], ring.to[1], side.to[0], side.to[1], side.other])
    for copy in local[:5]:
        copy.wait()
    for k in (0, 1):
        ring.start(0, k)
    local[5].wait()
    side.start()
    acc[...] = jnp.zeros_like(acc)
    local[6].wait()
    keep.start()

    def normalise():
        tile = 16

        def one(i, carry):
            slot, r = i // (rows // tile), lax.rem(i, rows // tile)
            v = raw[slot, pl.ds(pl.multiple_of(r * tile, tile), tile), :].astype(F32)
            v = v * lax.rsqrt(jnp.mean(v * v, axis=-1, keepdims=True) + EPS) * gain[...]
            v = v.astype(BF16)
            depth = nbuf.shape[2]
            for o in range(n):
                nbuf[o, pl.ds(pl.multiple_of(i * tile, tile), tile), :] = v[:, o * depth : (o + 1) * depth]
            return carry

        lax.fori_loop(0, raw.shape[0] * rows // tile, one, 0)

    def accumulate(o):
        tile = 256

        def one(i, carry):
            r = pl.ds(pl.multiple_of(i * tile, tile), tile)
            acc[r, :] += jnp.dot(nbuf[o, r, :], wbuf[o], preferred_element_type=F32)
            return carry

        lax.fori_loop(0, acc.shape[0] // tile, one, 0)

    last = n // 2 - 1
    ready = 2

    def spread(count):
        def one(i, carry):
            accumulate(lax.rem(me + n - count + i, n))
            return carry

        lax.fori_loop(0, 2 * count + 1, one, 0)

    def step(s, carry):
        ring.land(s, 0)
        ring.start(s + 1, 0)

        @pl.when(s == 0)
        def _():
            side.step(0)

        @pl.when(s == 1)
        def _():
            side.step(1)

        ring.land(s, 1)
        ring.start(s + 1, 1)

        @pl.when(s == 1)
        def _():
            side.step(2)
            late.start()

        @pl.when(s == ready)
        def _():
            side.finish()
            normalise()
            spread(ready + 1)

        @pl.when(s == 3)
        def _():
            late.step(0)

        @pl.when(s == 5)
        def _():
            late.step(1)

        @pl.when(s > ready)
        def _():
            accumulate(lax.rem(me + n - s - 1, n))
            accumulate(lax.rem(me + s + 1, n))

        return carry

    lax.fori_loop(0, last - 1, step, 0)
    ring.land(last - 1, 0)
    ring.start(last, 0)
    ring.land(last - 1, 1)
    late.step(2)
    accumulate(lax.rem(me + n - last, n))
    accumulate(lax.rem(me + last, n))
    ring.land(last, 0)
    accumulate(lax.rem(me + last + 1, n))
    at = 0
    for out in (kv_out, q_out, qw_out, kvw_out):
        out[...] = acc[:, at : at + out.shape[1]].astype(out.dtype)
        at += out.shape[1]
    late.finish()
    keep.wait()
    ring.drain()
    side.drain()
    late.drain()


def attend_kernel(
    n, q, kv, qw, kvw, lam, ogain, sink, pd, pwg, out,
    kbuf, kw, pdb, pwb, top, tot, acc, y, yd, yv, yw, facc,
    lsem, zs, zr, hs, hr, us, ur, ws, wr, *sems,
):
    me, x, c = (lax.axis_index(a) for a in ("sp", "tp_0", "tp_1"))
    t = 2 * x + c
    rows = q.shape[0]
    block = rows // (2 * NX)
    local = [
        pltpu.make_async_copy(kv, kbuf.at[me], lsem.at[0]),
        pltpu.make_async_copy(kvw, kw.at[c, pl.ds(WINDOW, rows)], lsem.at[1]),
        pltpu.make_async_copy(pd, pdb.at[t], lsem.at[2]),
        pltpu.make_async_copy(pwg, pwb, lsem.at[3]),
    ]
    for copy in local:
        copy.start()
    ring = Ring(n, kbuf, kbuf.shape[1] // 2, zs, zr)
    side = Side(None, pdb, pd.shape[0] // 2, *sems)

    def peer(k):
        return {"tp_0": lax.rem(x + k // 2, NX), "tp_1": lax.rem(c + k % 2, 2)}

    def slot(px, pc):
        return 2 * lax.rem(px, NX) + lax.rem(pc, 2)

    others = range(1, 2 * NX)
    greet([ring.to[0], ring.to[1]] + [peer(k) for k in others])

    def edge(d, inward):
        src = pl.ds(rows, WINDOW) if d == 0 else pl.ds(WINDOW, WINDOW)
        dst = pl.ds(0, WINDOW) if d == 0 else pl.ds(rows + WINDOW, WINDOW)
        target = kw.at[c, dst]
        return remote(target if inward else kw.at[c, src], target, hs.at[d], hr.at[d], ring.to[d])

    spans = (pl.ds(WINDOW, rows), pl.ds(0, WINDOW), pl.ds(rows + WINDOW, WINDOW))

    def twin(i, inward):
        ref = kw.at[1 - c if inward else c, spans[i]]
        return remote(ref, ref, us.at[i], ur.at[i], side.other)

    def trade(src, dst, send, recv, k, inward):
        if inward:
            ref = dst.at[slot(x + NX - k // 2, c + k % 2)]
            return remote(ref, ref, send.at[k], recv.at[k], peer(k))
        return remote(src.at[slot(x + k // 2, c + k % 2)], dst.at[t], send.at[k], recv.at[k], peer(k))

    local[0].wait()
    for k in (0, 1):
        ring.start(0, k)
    local[1].wait()
    for d in (0, 1):
        edge(d, False).start()
    twin(0, False).start()
    local[2].wait()
    side.start()

    top[...] = jnp.full_like(top, -jnp.inf)
    tot[...] = jnp.zeros_like(tot)
    acc[...] = jnp.zeros_like(acc)
    scale = HEAD**-0.5
    tile = 256
    lanes = HEAD
    contract_last = (((1,), (1,)), ((), ()))

    def attend(o):
        def one(i, carry):
            r = pl.ds(pl.multiple_of(i * tile, tile), tile)
            values = kbuf[o, :, 2 * HEAD :]
            for m in range(2):
                cols = pl.ds(m * HEAD, HEAD)
                s = lax.dot_general(q[r, cols], kbuf[o, :, cols], contract_last, preferred_element_type=F32)
                s = s * (scale * LOG2E)
                reps = s.shape[1] // lanes
                was = top[m, r, :]
                now = jnp.maximum(was, jnp.max(s, axis=1, keepdims=True))
                fade = jnp.exp2(was - now)
                e = jnp.exp2(s - jnp.concatenate([now] * reps, axis=1))
                part = e[:, :lanes]
                for j in range(1, reps):
                    part = part + e[:, j * lanes : (j + 1) * lanes]
                tot[m, r, :] = tot[m, r, :] * fade + part
                top[m, r, :] = now
                acc[m, r, :] = acc[m, r, :] * jnp.concatenate([fade] * (VDIM // lanes), axis=1) + jnp.dot(
                    e.astype(BF16), values, preferred_element_type=F32
                )
            return carry

        lax.fori_loop(0, rows // tile, one, 0)

    def window():
        span = 3 * WINDOW
        heads = qw.shape[1] // HEAD
        i_q = lax.broadcasted_iota(jnp.int32, (WINDOW, span), 0)
        i_k = lax.broadcasted_iota(jnp.int32, (WINDOW, span), 1)
        near = jnp.abs(i_k - WINDOW - i_q) <= WINDOW

        def one(b, carry):
            r = pl.ds(pl.multiple_of(b * WINDOW, WINDOW), WINDOW)
            band = pl.ds(pl.multiple_of(b * WINDOW, WINDOW), span)
            where = i_k + (me * rows + b * WINDOW - WINDOW)
            valid = near & (where >= 0) & (where < n * rows)
            for h in range(heads):
                cols = pl.ds(h * HEAD, HEAD)
                s = lax.dot_general(qw[r, cols], kw[0, band, :], contract_last, preferred_element_type=F32)
                s = jnp.where(valid, s * scale, -jnp.inf)
                sunk = jnp.broadcast_to(sink[h : h + 1, :], (WINDOW, lanes))
                peak = jnp.maximum(jnp.max(s, axis=1, keepdims=True), sunk)
                e = jnp.exp(s - jnp.concatenate([peak] * 3, axis=1))
                whole = jnp.sum(e, axis=1, keepdims=True) + jnp.exp(sunk - peak)
                w = (e / jnp.concatenate([whole] * 3, axis=1)).astype(BF16)
                res = jnp.dot(w, kw[1, band, :], preferred_element_type=F32).astype(BF16)
                for j in range(WINDOW // block):
                    yv[b * (WINDOW // block) + j, :, cols] = res[j * block : (j + 1) * block]
            return carry

        lax.fori_loop(0, rows // WINDOW, one, 0)

    width = 512

    def project(ys, weights, first):
        def one(j, carry):
            cols = pl.ds(pl.multiple_of(j * width, width), width)
            total = None if first else facc[:, cols]
            for i in range(2 * NX):
                p = jnp.dot(ys[i], weights[i, :, cols], preferred_element_type=F32)
                total = p if total is None else total + p
            if first:
                facc[:, cols] = total
            else:
                out[:, cols] = total.astype(out.dtype)
            return carry

        lax.fori_loop(0, out.shape[1] // width, one, 0)

    attend(me)
    last = n // 2 - 1

    def step(s, carry):
        ring.land(s, 0)
        ring.start(s + 1, 0)

        @pl.when(s == 0)
        def _():
            for d in (0, 1):
                edge(d, True).wait_recv()
                twin(d + 1, False).start()

        @pl.when(s > 0)
        def _():
            attend(ring.origin(0, s))

        ring.land(s, 1)
        ring.start(s + 1, 1)

        @pl.when(s > 0)
        def _():
            attend(ring.origin(1, s))

        @pl.when(s == 1)
        def _():
            for i in range(3):
                twin(i, True).wait_recv()
            window()
            yw[t] = yv[t]

        @pl.when(s == 2)
        def _():
            for k in others:
                trade(yv, yw, ws, wr, k, False).start()
            side.step(0)

        @pl.when(s == 4)
        def _():
            local[3].wait()
            for k in others:
                trade(yv, yw, ws, wr, k, True).wait_recv()
            project(yw, pwb, True)
            side.step(1)

        return carry

    lax.fori_loop(0, last - 1, step, 0)
    ring.land(last - 1, 0)
    ring.start(last, 0)
    attend(ring.origin(0, last - 1))
    ring.land(last - 1, 1)
    attend(ring.origin(1, last - 1))
    side.step(2)

    def both(i, carry):
        attend(lax.rem(me + n - last + 2 * last * i, n))
        return carry

    lax.fori_loop(0, 2, both, 0)
    side.finish()
    ring.land(last, 0)
    attend(lax.rem(me + last + 1, n))

    def close(j, carry):
        r = pl.ds(pl.multiple_of(j * block, block), block)
        maps = [acc[m, r, :] / jnp.sum(tot[m, r, :], axis=1, keepdims=True) for m in range(2)]
        d = maps[0] - lam[...] * maps[1]
        d = d * lax.rsqrt(jnp.mean(d * d, axis=-1, keepdims=True) + EPS) * ogain[...]
        y[j] = d.astype(BF16)
        return carry

    lax.fori_loop(0, 2 * NX, close, 0)
    for k in others:
        trade(y, yd, us.at[pl.ds(3, 2 * NX)], ur.at[pl.ds(3, 2 * NX)], k, False).start()
    yd[t] = y[t]
    for k in others:
        trade(y, yd, us.at[pl.ds(3, 2 * NX)], ur.at[pl.ds(3, 2 * NX)], k, True).wait_recv()
    project(yd, pdb, False)
    for k in others:
        trade(y, yd, us.at[pl.ds(3, 2 * NX)], ur.at[pl.ds(3, 2 * NX)], k, False).wait_send()
        trade(yv, yw, ws, wr, k, False).wait_send()
    for d in (0, 1):
        edge(d, False).wait_send()
    for i in range(3):
        twin(i, False).wait_send()
    ring.drain()
    side.drain()


def call(kernel, ins, outs, scratch, ident, args):
    return pl.pallas_call(
        kernel,
        out_shape=[s for s, _ in outs],
        in_specs=[pl.BlockSpec(memory_space=m) for m in ins],
        out_specs=[pl.BlockSpec(memory_space=m) for _, m in outs],
        scratch_shapes=scratch,
        compiler_params=pltpu.CompilerParams(
            collective_id=ident, has_side_effects=True, vmem_limit_bytes=64_000_000
        ),
    )(*args)


def body(
    n, tokens, norm_gain, query_diff, key_diff, value_diff, lam, output_norm_gain,
    query_win, keyval_win, sink, proj_diff, proj_win,
):
    block, model = tokens.shape
    rows = block * 2 * NX
    depth = query_diff.shape[0]
    kvd = key_diff.shape[1] + value_diff.shape[1]
    part = keyval_win.shape[2] // 2
    wide = kvd + query_diff.shape[1] + query_win.shape[1] + part
    heads_win = sink.shape[0]
    shape = jax.ShapeDtypeStruct
    kv, q, qw, kvw, pwg = call(
        functools.partial(project_kernel, n, heads_win),
        [ANY, VMEM] + [ANY] * 6,
        [
            (shape((rows, kvd), BF16), VMEM),
            (shape((rows, query_diff.shape[1]), BF16), VMEM),
            (shape((rows, query_win.shape[1]), BF16), VMEM),
            (shape((rows, part), BF16), VMEM),
            (shape((2 * NX,) + proj_win.shape, BF16), ANY),
        ],
        [
            VMEM((n, depth, wide), BF16),
            VMEM((2 * NX, block, model), BF16),
            VMEM((n, rows, depth), BF16),
            VMEM((rows, wide), F32),
            VMEM(proj_win.shape, BF16),
            DMA((8,)),
            DMA((2, n // 2, 2)),
            DMA((2, n // 2, 2)),
        ]
        + side_sems()
        + side_sems(),
        0,
        (
            tokens, norm_gain.reshape(1, model), key_diff, value_diff, query_diff, query_win,
            keyval_win, proj_win,
        ),
    )
    (mixed,) = call(
        functools.partial(attend_kernel, n),
        [VMEM, ANY, VMEM, ANY, VMEM, VMEM, VMEM, ANY, ANY],
        [(shape((block, model), BF16), VMEM)],
        [
            VMEM((n, rows, kvd), BF16),
            VMEM((2, rows + 2 * WINDOW, part), BF16),
            VMEM((2 * NX,) + proj_diff.shape, BF16),
            VMEM((2 * NX,) + proj_win.shape, BF16),
            VMEM((2, rows, HEAD), F32),
            VMEM((2, rows, HEAD), F32),
            VMEM((2, rows, VDIM), F32),
            VMEM((2 * NX, block, VDIM), BF16),
            VMEM((2 * NX, block, VDIM), BF16),
            VMEM((2 * NX, block, query_win.shape[1]), BF16),
            VMEM((2 * NX, block, query_win.shape[1]), BF16),
            VMEM((block, model), F32),
            DMA((4,)),
            DMA((2, n // 2, 2)),
            DMA((2, n // 2, 2)),
            DMA((2,)),
            DMA((2,)),
            DMA((3 + 2 * NX,)),
            DMA((3 + 2 * NX,)),
            DMA((2 * NX,)),
            DMA((2 * NX,)),
        ]
        + side_sems(),
        1,
        (
            q, kv, qw, kvw,
            jnp.broadcast_to(lam[:, None], (1, VDIM)),
            output_norm_gain.reshape(1, VDIM),
            jnp.broadcast_to(sink[:, None], (heads_win, HEAD)),
            proj_diff, pwg,
        ),
    )
    return mixed


def solution(mesh):
    torus = Mesh(
        mesh.devices.reshape(mesh.shape["grp"], mesh.shape["sp"], NX, 2),
        ("grp", "sp", "tp_0", "tp_1"),
    )
    return jax.shard_map(
        functools.partial(body, mesh.shape["sp"]),
        mesh=torus,
        in_specs=(
            P(GRP_SP_TP, None),
            P(),
            P("sp", TP),
            P("sp", TP),
            P("sp", TP),
            P(TP),
            P(),
            P("sp", TP),
            P(None, "sp", None),
            P(TP),
            P(TP, None),
            P(TP, None),
        ),
        out_specs=P(GRP_SP_TP, None),
        check_vma=False,
    )
```

time: 443 us -> 239 us (0.54)
  waiting for transfers between devices: 331 us -> 0 us
  Pallas kernels: 0 us -> 234 us
  matrix products: 38.1 us -> 0 us
  local copies, waits for them, and re-layouts: 41.4 us -> 3.73 us
  between operations: 14.2 us -> 0.67 us
  other arithmetic: 12.5 us -> 0 us
    all_gather x4 -> x0, waiting for transfers between devices: 289 us -> none  [the longest x1 122 us: body(): lax.all_gather(stacked, 'sp', axis=0, tiled=True)]
    pallas_call x0 -> x2, Pallas kernels: none -> 234 us  [call(): pl.pallas_call(kernel, out_shape=[s for s, _ in outs], in_specs=[pl.Block...]
    reduce_scatter x1 -> x0, waiting for transfers between devices: 40.1 us -> none  [body(): lax.psum_scatter((summed + jnp.dot(y_win, proj_win, preferred_element_typ...]
    dot_general x21 -> x0, matrix products: 38.1 us -> none  [the longest x8 16.5 us: one(): jnp.einsum('hmqk,khe->hmqe', expo.astype(jnp.bfloat16), value_part, prefe...]
    dynamic_slice x8 -> x0, local copies, waits for them, and re-layouts: 11.2 us -> none  [body(): carry, unused = lax.scan(one, carry, (key_blocks, value_blocks))]
    while x40 -> x0, local copies, waits for them, and re-layouts: 7.65 us -> none
    slice x3 -> x0, local copies, waits for them, and re-layouts: 7.6 us -> none  [the longest x1 5.73 us: side_by_side(): done.append(lax.slice_in_dim(out, at, at + a.shape[along], axis=along))]
    reduce_sum x11 -> x0, other arithmetic: 7.38 us -> none  [the longest x8 5.6 us: one(): total = total * fade + jnp.sum(expo, axis=-1)]
  transfers between devices with their start and end apart: 7 -> 0, of which waited for: 6 -> 0; matrix products, arithmetic and copies ran while one was open for 2% -> 0% of each run, Pallas kernels for 0% -> 0%
where the time goes in v1:
time: 239 us
  Pallas kernels  234 us (98%)
  local copies, waits for them, and re-layouts  3.73 us (2%)
    pallas_call x2, Pallas kernels, call(): pl.pallas_call(kernel, out_shape=[s for s, _ in outs], in_specs=[pl.Block...  234 us

profile of v1, /device:TPU:33, one launch (start us, length us, event | category | flops | bytes accessed | tf_op | source)
XLA Modules:
  0.0 238.6 jit_solution(1221861681423504561)
XLA Ops:
  0.7 0.6 broadcast_in_dim.7.lam
  1.2 1.3 broadcast_in_dim.16.sink
  2.5 129.0 %shard_map.118 = (bf16[512,512]{1,0:T(8,128)(2,1)}, bf16[512,256]{1,0:T(8,128)(2,1)}, bf16[512,256]{1,0:T(8,128)(2,1)}, bf16[512,128]{1,0:T(8,128)(2,1)}, bf16[8,256,4096]{2,1,0:T(8,128)(2,1)}) custom-call(bf16[64,4096]{1,0:T(8,128)(2,1)} %tok.1, f32[1,4096]{1,0:T(1,128)} %bitcast.4, bf16[256,256]{1,0:T(8,128)(2,1)} %kd.1, bf16[256,256]{1,0:T(8,128)(2,1)} %vd.1, ...), custom_call_target="tpu_custom_call" | custom-call | tf_op jit(solution)/shard_map/pallas_call | solution.py:527
  131.5 105.2 %shard_map.119 = bf16[64,4096]{1,0:T(8,128)(2,1)} custom-call(bf16[512,256]{1,0:T(8,128)(2,1)} %get-tuple-element.10.q, bf16[512,512]{1,0:T(8,128)(2,1)} %get-tuple-element.11.kv, bf16[512,256]{1,0:T(8,128)(2,1)} %get-tuple-element.12.qw, bf16[512,128]{1,0:T(8,128)(2,1)} %get-tuple-element.13.kvw, f32[1,256]{1,0:T(1,128)} %broadcast_in_dim.7.lam, ...), custom_call_target="tpu_custom_call" | custom-call | tf_op jit(solution)/shard_map/pallas_call | solution.py:527
  236.7 1.9 copy.15

commit v2 on v1

--- a/solution.py
+++ b/solution.py
@@ -14,6 +14,7 @@
 WINDOW = 128
 VDIM = 256
 NX = 4
+CUT = 80
 TP = ("tp_0", "tp_1")
 GRP_SP_TP = ("grp", "sp", "tp_0", "tp_1")
 EPS = 1e-06
@@ -45,8 +46,9 @@
 
 
 class Ring:
-    def __init__(self, n, buf, half, send, recv):
-        self.n, self.buf, self.half, self.send, self.recv = n, buf, half, send, recv
+    def __init__(self, n, buf, base, cuts, send, recv):
+        self.n, self.buf, self.send, self.recv = n, buf, send, recv
+        self.spans = (pl.ds(base, cuts[0]), pl.ds(base + cuts[0], cuts[1]))
         self.me = lax.axis_index("sp")
         self.to = (
             {"sp": lax.rem(self.me + 1, n)},
@@ -57,8 +59,7 @@
         return lax.rem(self.me + (self.n - s if d == 0 else s), self.n)
 
     def piece(self, d, s, k, hops):
-        b = k if d == 0 else 1 - k
-        ref = self.buf.at[self.origin(d, hops), pl.ds(b * self.half, self.half)]
+        ref = self.buf.at[self.origin(d, hops), self.spans[k if d == 0 else 1 - k]]
         return remote(ref, ref, self.send.at[d, s, k], self.recv.at[d, s, k], self.to[d])
 
     def start(self, s, k):
@@ -81,6 +82,33 @@
         lax.fori_loop(0, last, one, 0)
         for d in (0, 1):
             self.piece(d, last, 0, last).wait_send()
+
+
+class Swap:
+    def __init__(self, n, buf, cut, send, recv):
+        self.n, self.buf, self.cut, self.send, self.recv = n, buf, cut, send, recv
+        g = lax.axis_index("grp")
+        self.odd = lax.rem(g, 2)
+        self.to = {"grp": g + 1 - 2 * self.odd}
+        self.kept = buf.shape[1] - cut
+        self.base = pl.multiple_of(self.odd * cut, 16)
+
+    def piece(self, o, odd):
+        ref = self.buf.at[o, pl.ds(pl.multiple_of(odd * self.kept, 16), self.cut)]
+        return remote(ref, ref, self.send.at[o], self.recv.at[o], self.to)
+
+    def start(self, o):
+        self.piece(o, self.odd).start()
+
+    def land(self, o):
+        self.piece(o, 1 - self.odd).wait_recv()
+
+    def drain(self):
+        def one(i, carry):
+            self.piece(lax.rem(lax.axis_index("sp") + i, self.n), self.odd).wait_send()
+            return carry
+
+        lax.fori_loop(1, self.n, one, 0)
 
 
 class Side:
@@ -160,9 +188,9 @@
 
 
 def project_kernel(
-    n, heads_win, tok, gain, kd, vd, qd, qw, kvw, pw,
-    kv_out, q_out, qw_out, kvw_out, pw_out,
-    wbuf, raw, nbuf, acc, hold, lsem, zs, zr, *sems,
+    n, heads_win, tok, gain, kd, vd, qd, qw, kvw,
+    kv_out, q_out, qw_out, kvw_out,
+    wbuf, raw, nbuf, acc, lsem, zs, zr, ys, yr, *sems,
 ):
     me, x, c = (lax.axis_index(a) for a in ("sp", "tp_0", "tp_1"))
     t = 2 * x + c
@@ -181,17 +209,15 @@
         )
     )
     local.append((tok, raw.at[t]))
-    local.append((pw, hold))
     local = [pltpu.make_async_copy(a, b, lsem.at[i]) for i, (a, b) in enumerate(local)]
     for copy in local:
         copy.start()
-    keep = pltpu.make_async_copy(hold, pw_out.at[t], lsem.at[len(local)])
-
-    ring = Ring(n, wbuf, wbuf.shape[1] // 2, zs, zr)
+
+    swap = Swap(n, wbuf, CUT, ys, yr)
+    ring = Ring(n, wbuf, swap.base, (96, swap.kept - 96), zs, zr)
     rows = raw.shape[1]
-    side = Side(None, raw, rows // 2, *sems[:4])
-    late = Side(pw, pw_out, pw.shape[0] // 2, *sems[4:])
-    greet([ring.to[0], ring.to[1], side.to[0], side.to[1], side.other])
+    side = Side(None, raw, rows // 2, *sems)
+    greet([ring.to[0], ring.to[1], side.to[0], side.to[1], side.other, swap.to])
     for copy in local[:5]:
         copy.wait()
     for k in (0, 1):
@@ -199,8 +225,6 @@
     local[5].wait()
     side.start()
     acc[...] = jnp.zeros_like(acc)
-    local[6].wait()
-    keep.start()
 
     def normalise():
         tile = 16
@@ -220,6 +244,10 @@
     def accumulate(o):
         tile = 256
 
+        @pl.when(o != me)
+        def _():
+            swap.land(o)
+
         def one(i, carry):
             r = pl.ds(pl.multiple_of(i * tile, tile), tile)
             acc[r, :] += jnp.dot(nbuf[o, r, :], wbuf[o], preferred_element_type=F32)
@@ -228,7 +256,7 @@
         lax.fori_loop(0, acc.shape[0] // tile, one, 0)
 
     last = n // 2 - 1
-    ready = 2
+    ready = 3
 
     def spread(count):
         def one(i, carry):
@@ -241,66 +269,67 @@
         ring.land(s, 0)
         ring.start(s + 1, 0)
 
-        @pl.when(s == 0)
+        @pl.when(s == 1)
         def _():
             side.step(0)
 
-        @pl.when(s == 1)
+        @pl.when(s == 2)
         def _():
             side.step(1)
+
+        @pl.when(s > ready)
+        def _():
+            accumulate(ring.origin(0, s))
 
         ring.land(s, 1)
         ring.start(s + 1, 1)
-
-        @pl.when(s == 1)
+        for d in (0, 1):
+            swap.start(ring.origin(d, s + 1))
+
+        @pl.when(s == 2)
         def _():
             side.step(2)
-            late.start()
 
         @pl.when(s == ready)
         def _():
             side.finish()
             normalise()
-            spread(ready + 1)
-
-        @pl.when(s == 3)
-        def _():
-            late.step(0)
-
-        @pl.when(s == 5)
-        def _():
-            late.step(1)
+            spread(ready)
 
         @pl.when(s > ready)
         def _():
-            accumulate(lax.rem(me + n - s - 1, n))
-            accumulate(lax.rem(me + s + 1, n))
+            accumulate(ring.origin(1, s))
 
         return carry
 
     lax.fori_loop(0, last - 1, step, 0)
     ring.land(last - 1, 0)
     ring.start(last, 0)
+    accumulate(ring.origin(0, last - 1))
     ring.land(last - 1, 1)
-    late.step(2)
-    accumulate(lax.rem(me + n - last, n))
-    accumulate(lax.rem(me + last, n))
+    for d in (0, 1):
+        swap.start(ring.origin(d, last))
+    accumulate(ring.origin(1, last - 1))
     ring.land(last, 0)
-    accumulate(lax.rem(me + last + 1, n))
+    swap.start(ring.origin(0, last + 1))
+
+    def rest(i, carry):
+        accumulate(lax.rem(me + jnp.where(i == 0, n - last, last + i - 1), n))
+        return carry
+
+    lax.fori_loop(0, 3, rest, 0)
     at = 0
     for out in (kv_out, q_out, qw_out, kvw_out):
         out[...] = acc[:, at : at + out.shape[1]].astype(out.dtype)
         at += out.shape[1]
-    late.finish()
-    keep.wait()
     ring.drain()
+    swap.drain()
     side.drain()
-    late.drain()
 
 
 def attend_kernel(
-    n, q, kv, qw, kvw, lam, ogain, sink, pd, pwg, out,
-    kbuf, kw, pdb, pwb, top, tot, acc, y, yd, yv, yw, facc,
+    n, q, kv, qw, kvw, lam, ogain, sink, pd, pw, out,
+    kbuf, kw, pdb, top, tot, acc, y, yd, yv, give, take, sums,
     lsem, zs, zr, hs, hr, us, ur, ws, wr, *sems,
 ):
     me, x, c = (lax.axis_index(a) for a in ("sp", "tp_0", "tp_1"))
@@ -311,11 +340,10 @@
         pltpu.make_async_copy(kv, kbuf.at[me], lsem.at[0]),
         pltpu.make_async_copy(kvw, kw.at[c, pl.ds(WINDOW, rows)], lsem.at[1]),
         pltpu.make_async_copy(pd, pdb.at[t], lsem.at[2]),
-        pltpu.make_async_copy(pwg, pwb, lsem.at[3]),
     ]
     for copy in local:
         copy.start()
-    ring = Ring(n, kbuf, kbuf.shape[1] // 2, zs, zr)
+    ring = Ring(n, kbuf, 0, (kbuf.shape[1] // 2,) * 2, zs, zr)
     side = Side(None, pdb, pd.shape[0] // 2, *sems)
 
     def peer(k):
@@ -344,6 +372,12 @@
             ref = dst.at[slot(x + NX - k // 2, c + k % 2)]
             return remote(ref, ref, send.at[k], recv.at[k], peer(k))
         return remote(src.at[slot(x + k // 2, c + k % 2)], dst.at[t], send.at[k], recv.at[k], peer(k))
+
+    pass_on = remote(give, take, ws.at[0], wr.at[0], side.other)
+
+    def deal(k, inward):
+        to = lax.rem(x + k, NX)
+        return remote(sums.at[k - 1] if inward else take.at[to], sums.at[k - 1], ws.at[k], wr.at[k], {"tp_0": to})
 
     local[0].wait()
     for k in (0, 1):
@@ -411,27 +445,37 @@
                 w = (e / jnp.concatenate([whole] * 3, axis=1)).astype(BF16)
                 res = jnp.dot(w, kw[1, band, :], preferred_element_type=F32).astype(BF16)
                 for j in range(WINDOW // block):
-                    yv[b * (WINDOW // block) + j, :, cols] = res[j * block : (j + 1) * block]
+                    yv[j % 2, b * (WINDOW // block // 2) + j // 2, :, cols] = res[j * block : (j + 1) * block]
             return carry
 
         lax.fori_loop(0, rows // WINDOW, one, 0)
 
     width = 512
 
-    def project(ys, weights, first):
-        def one(j, carry):
-            cols = pl.ds(pl.multiple_of(j * width, width), width)
-            total = None if first else facc[:, cols]
-            for i in range(2 * NX):
-                p = jnp.dot(ys[i], weights[i, :, cols], preferred_element_type=F32)
-                total = p if total is None else total + p
-            if first:
-                facc[:, cols] = total
-            else:
-                out[:, cols] = total.astype(out.dtype)
-            return carry
-
-        lax.fori_loop(0, out.shape[1] // width, one, 0)
+    def columns(one):
+        def run(j, carry):
+            one(pl.ds(pl.multiple_of(j * width, width), width))
+            return carry
+
+        lax.fori_loop(0, out.shape[1] // width, run, 0)
+
+    def window_rows(core, cols):
+        ys = yv[core].reshape(NX * block, yv.shape[3])
+        return jnp.dot(ys, pw[:, cols], preferred_element_type=F32).reshape(NX, block, width)
+
+    def to_give(cols):
+        give[:, :, cols] = window_rows(1 - c, cols).astype(BF16)
+
+    def to_sum(cols):
+        take[:, :, cols] = (window_rows(c, cols) + take[:, :, cols].astype(F32)).astype(BF16)
+
+    def to_out(cols):
+        total = take[x, :, cols].astype(F32)
+        for k in range(1, NX):
+            total = total + sums[k - 1, :, cols].astype(F32)
+        for i in range(2 * NX):
+            total = total + jnp.dot(yd[i], pdb[i, :, cols], preferred_element_type=F32)
+        out[:, cols] = total.astype(out.dtype)
 
     attend(me)
     last = n // 2 - 1
@@ -462,20 +506,22 @@
             for i in range(3):
                 twin(i, True).wait_recv()
             window()
-            yw[t] = yv[t]
 
         @pl.when(s == 2)
         def _():
-            for k in others:
-                trade(yv, yw, ws, wr, k, False).start()
             side.step(0)
+            columns(to_give)
+            pass_on.start()
+
+        @pl.when(s == 3)
+        def _():
+            pass_on.wait_recv()
+            columns(to_sum)
 
         @pl.when(s == 4)
         def _():
-            local[3].wait()
-            for k in others:
-                trade(yv, yw, ws, wr, k, True).wait_recv()
-            project(yw, pwb, True)
+            for k in range(1, NX):
+                deal(k, False).start()
             side.step(1)
 
         return carry
@@ -494,6 +540,8 @@
 
     lax.fori_loop(0, 2, both, 0)
     side.finish()
+    for k in range(1, NX):
+        deal(k, True).wait_recv()
     ring.land(last, 0)
     attend(lax.rem(me + last + 1, n))
 
@@ -511,14 +559,16 @@
     yd[t] = y[t]
     for k in others:
         trade(y, yd, us.at[pl.ds(3, 2 * NX)], ur.at[pl.ds(3, 2 * NX)], k, True).wait_recv()
-    project(yd, pdb, False)
+    columns(to_out)
     for k in others:
         trade(y, yd, us.at[pl.ds(3, 2 * NX)], ur.at[pl.ds(3, 2 * NX)], k, False).wait_send()
-        trade(yv, yw, ws, wr, k, False).wait_send()
     for d in (0, 1):
         edge(d, False).wait_send()
     for i in range(3):
         twin(i, False).wait_send()
+    pass_on.wait_send()
+    for k in range(1, NX):
+        deal(k, False).wait_send()
     ring.drain()
     side.drain()
 
@@ -548,60 +598,59 @@
     wide = kvd + query_diff.shape[1] + query_win.shape[1] + part
     heads_win = sink.shape[0]
     shape = jax.ShapeDtypeStruct
-    kv, q, qw, kvw, pwg = call(
+    kv, q, qw, kvw = call(
         functools.partial(project_kernel, n, heads_win),
-        [ANY, VMEM] + [ANY] * 6,
+        [ANY, VMEM] + [ANY] * 5,
         [
             (shape((rows, kvd), BF16), VMEM),
             (shape((rows, query_diff.shape[1]), BF16), VMEM),
             (shape((rows, query_win.shape[1]), BF16), VMEM),
             (shape((rows, part), BF16), VMEM),
-            (shape((2 * NX,) + proj_win.shape, BF16), ANY),
         ],
         [
             VMEM((n, depth, wide), BF16),
             VMEM((2 * NX, block, model), BF16),
             VMEM((n, rows, depth), BF16),
             VMEM((rows, wide), F32),
-            VMEM(proj_win.shape, BF16),
-            DMA((8,)),
+            DMA((6,)),
             DMA((2, n // 2, 2)),
             DMA((2, n // 2, 2)),
+            DMA((n,)),
+            DMA((n,)),
         ]
-        + side_sems()
         + side_sems(),
         0,
         (
             tokens, norm_gain.reshape(1, model), key_diff, value_diff, query_diff, query_win,
-            keyval_win, proj_win,
+            keyval_win,
         ),
     )
     (mixed,) = call(
         functools.partial(attend_kernel, n),
-        [VMEM, ANY, VMEM, ANY, VMEM, VMEM, VMEM, ANY, ANY],
+        [VMEM, ANY, VMEM, ANY, VMEM, VMEM, VMEM, ANY, VMEM],
         [(shape((block, model), BF16), VMEM)],
         [
             VMEM((n, rows, kvd), BF16),
             VMEM((2, rows + 2 * WINDOW, part), BF16),
             VMEM((2 * NX,) + proj_diff.shape, BF16),
-            VMEM((2 * NX,) + proj_win.shape, BF16),
             VMEM((2, rows, HEAD), F32),
             VMEM((2, rows, HEAD), F32),
             VMEM((2, rows, VDIM), F32),
             VMEM((2 * NX, block, VDIM), BF16),
             VMEM((2 * NX, block, VDIM), BF16),
-            VMEM((2 * NX, block, query_win.shape[1]), BF16),
-            VMEM((2 * NX, block, query_win.shape[1]), BF16),
-            VMEM((block, model), F32),
-            DMA((4,)),
+            VMEM((2, NX, block, query_win.shape[1]), BF16),
+            VMEM((NX, block, model), BF16),
+            VMEM((NX, block, model), BF16),
+            VMEM((NX - 1, block, model), BF16),
+            DMA((3,)),
             DMA((2, n // 2, 2)),
             DMA((2, n // 2, 2)),
             DMA((2,)),
             DMA((2,)),
             DMA((3 + 2 * NX,)),
             DMA((3 + 2 * NX,)),
-            DMA((2 * NX,)),
-            DMA((2 * NX,)),
+            DMA((NX,)),
+            DMA((NX,)),
         ]
         + side_sems(),
         1,
@@ -610,7 +659,7 @@
             jnp.broadcast_to(lam[:, None], (1, VDIM)),
             output_norm_gain.reshape(1, VDIM),
             jnp.broadcast_to(sink[:, None], (heads_win, HEAD)),
-            proj_diff, pwg,
+            proj_diff, proj_win,
         ),
     )
     return mixed

time: 239 us -> 223 us (0.933)
  Pallas kernels: 234 us -> 218 us
    pallas_call x2, Pallas kernels: 234 us -> 218 us  [call(): pl.pallas_call(kernel, out_shape=[s for s, _ in outs], in_specs=[pl.Block...]
where the time goes in v2:
time: 223 us; the launch traced here: 222 us
  Pallas kernels  218 us (98%)
  local copies, waits for them, and re-layouts  3.73 us (2%)
    pallas_call x2, Pallas kernels, call(): pl.pallas_call(kernel, out_shape=[s for s, _ in outs], in_specs=[pl.Block...  218 us

profile of v2, /device:TPU:33, one launch (start us, length us, event | category | flops | bytes accessed | tf_op | source)
XLA Modules:
  0.0 222.3 jit_solution(15048987893994036794)
XLA Ops:
  0.7 0.6 broadcast_in_dim.7.lam
  1.2 1.3 broadcast_in_dim.16.sink
  2.5 102.1 %shard_map.118 = (bf16[512,512]{1,0:T(8,128)(2,1)}, bf16[512,256]{1,0:T(8,128)(2,1)}, bf16[512,256]{1,0:T(8,128)(2,1)}, bf16[512,128]{1,0:T(8,128)(2,1)}) custom-call(bf16[64,4096]{1,0:T(8,128)(2,1)} %tok.1, f32[1,4096]{1,0:T(1,128)} %bitcast.4, bf16[256,256]{1,0:T(8,128)(2,1)} %kd.1, bf16[256,256]{1,0:T(8,128)(2,1)} %vd.1, bf16[256,256]{1,0:T(8,128)(2,1)} %qd.1, ...), custom_call_target="tpu_custom_call" | custom-call | tf_op jit(solution)/shard_map/pallas_call | solution.py:577
  104.6 115.8 %shard_map.119 = bf16[64,4096]{1,0:T(8,128)(2,1)} custom-call(bf16[512,256]{1,0:T(8,128)(2,1)} %get-tuple-element.9.q, bf16[512,512]{1,0:T(8,128)(2,1)} %get-tuple-element.10.kv, bf16[512,256]{1,0:T(8,128)(2,1)} %get-tuple-element.11.qw, bf16[512,128]{1,0:T(8,128)(2,1)} %get-tuple-element.12.kvw, f32[1,256]{1,0:T(1,128)} %broadcast_in_dim.7.lam, ...), custom_call_target="tpu_custom_call" | custom-call | tf_op jit(solution)/shard_map/pallas_call | solution.py:577
  220.5 1.9 copy.15

commit v3 on v2

v3 whole, which is shorter than its diff:
```python
import functools

import jax
import jax.numpy as jnp
from jax import lax
from jax.experimental import pallas as pl
from jax.experimental.pallas import tpu as pltpu
from jax.sharding import Mesh
from jax.sharding import PartitionSpec as P

HEAD = 128
WIN_HEADS = 16
KV_HEADS = 4
WINDOW = 128
VDIM = 256
NX = 4
CUT = 80
TP = ("tp_0", "tp_1")
GRP_SP_TP = ("grp", "sp", "tp_0", "tp_1")
EPS = 1e-06
LOG2E = 1.4426950408889634
BF16 = jnp.bfloat16
F32 = jnp.float32
MESH = pl.DeviceIdType.MESH
DMA = pltpu.SemaphoreType.DMA
VMEM = pltpu.VMEM
ANY = pl.ANY


def remote(src, dst, send_sem, recv_sem, where):
    return pltpu.make_async_remote_copy(
        src_ref=src,
        dst_ref=dst,
        send_sem=send_sem,
        recv_sem=recv_sem,
        device_id=where,
        device_id_type=MESH,
    )


def greet(peers):
    barrier = pltpu.get_barrier_semaphore()
    for peer in peers:
        pl.semaphore_signal(barrier, inc=1, device_id=peer, device_id_type=MESH)
    pl.semaphore_wait(barrier, len(peers))


class Ring:
    def __init__(self, n, buf, base, cuts, send, recv):
        self.n, self.buf, self.send, self.recv = n, buf, send, recv
        self.spans = []
        for cut in cuts:
            self.spans.append(pl.ds(base, cut))
            base = base + cut
        self.count = len(cuts)
        self.me = lax.axis_index("sp")
        self.to = (
            {"sp": lax.rem(self.me + 1, n)},
            {"sp": lax.rem(self.me + n - 1, n)},
        )

    def origin(self, d, s):
        return lax.rem(self.me + (self.n - s if d == 0 else s), self.n)

    def piece(self, d, s, k, hops):
        ref = self.buf.at[self.origin(d, hops), self.spans[k if d == 0 else self.count - 1 - k]]
        return remote(ref, ref, self.send.at[d, s, k], self.recv.at[d, s, k], self.to[d])

    def start(self, s, k):
        for d in (0, 1):
            self.piece(d, s, k, s).start()

    def land(self, s, k):
        for d in (0, 1):
            self.piece(d, s, k, s + 1).wait_recv()

    def drain(self):
        last = self.n // 2 - 1

        def one(s, carry):
            for k in range(self.count):
                for d in (0, 1):
                    self.piece(d, s, k, s).wait_send()
            return carry

        lax.fori_loop(0, last, one, 0)
        for k in range(self.count // 2):
            for d in (0, 1):
                self.piece(d, last, k, last).wait_send()


class Swap:
    def __init__(self, n, buf, cut, send, recv):
        self.n, self.buf, self.cut, self.send, self.recv = n, buf, cut, send, recv
        g = lax.axis_index("grp")
        self.odd = lax.rem(g, 2)
        self.to = {"grp": g + 1 - 2 * self.odd}
        self.kept = buf.shape[1] - cut
        self.base = pl.multiple_of(self.odd * cut, 16)

    def piece(self, o, odd):
        ref = self.buf.at[o, pl.ds(pl.multiple_of(odd * self.kept, 16), self.cut)]
        return remote(ref, ref, self.send.at[o], self.recv.at[o], self.to)

    def start(self, o):
        self.piece(o, self.odd).start()

    def land(self, o):
        self.piece(o, 1 - self.odd).wait_recv()

    def drain(self):
        def one(i, carry):
            self.piece(lax.rem(lax.axis_index("sp") + i, self.n), self.odd).wait_send()
            return carry

        lax.fori_loop(1, self.n, one, 0)


class Side:
    def __init__(self, own, slots, half, xs, xr, cs, cr):
        self.own, self.slots, self.half = own, slots, half
        self.xs, self.xr, self.cs, self.cr = xs, xr, cs, cr
        self.x = lax.axis_index("tp_0")
        self.c = lax.axis_index("tp_1")
        self.to = (
            {"tp_0": lax.rem(self.x + 1, NX)},
            {"tp_0": lax.rem(self.x + NX - 1, NX)},
        )
        self.other = {"tp_1": 1 - self.c}

    def spot(self, rel, h, core):
        slot = 2 * lax.rem(self.x + rel, NX) + core
        return self.slots.at[slot, pl.ds(h * self.half, self.half)]

    def source(self, rel, h):
        if rel == 0 and self.own is not None:
            return self.own.at[pl.ds(h * self.half, self.half)]
        return self.spot(rel, h, self.c)

    def half_of(self, d, k):
        return (0, 1, 0)[k] if d == 0 else (1, 0, 1)[k]

    def out(self, d, k):
        rel = 0 if k < 2 else (3 if d == 0 else 1)
        h = self.half_of(d, k)
        return remote(
            self.source(rel, h), self.spot(rel, h, self.c), self.xs.at[d, k], self.xr.at[d, k], self.to[d]
        )

    def inward(self, d, k):
        rel = (3 if d == 0 else 1) if k < 2 else 2
        h = self.half_of(d, k)
        ref = self.spot(rel, h, self.c)
        return rel, h, remote(ref, ref, self.xs.at[d, k], self.xr.at[d, k], self.to[d])

    def across(self, rel, h):
        return remote(
            self.source(rel, h), self.spot(rel, h, self.c), self.cs.at[rel, h], self.cr.at[rel, h], self.other
        )

    def start(self):
        for k in (0, 1):
            for d in (0, 1):
                self.out(d, k).start()
        for h in (0, 1):
            self.across(0, h).start()

    def step(self, k):
        for d in (0, 1):
            rel, h, copy = self.inward(d, k)
            copy.wait_recv()
            if k == 0:
                self.out(d, 2).start()
            self.across(rel, h).start()

    def finish(self):
        for rel in range(NX):
            for h in (0, 1):
                ref = self.spot(rel, h, 1 - self.c)
                remote(ref, ref, self.cs.at[rel, h], self.cr.at[rel, h], self.other).wait_recv()

    def drain(self):
        for k in (0, 1, 2):
            for d in (0, 1):
                self.out(d, k).wait_send()
        for rel in range(NX):
            for h in (0, 1):
                self.across(rel, h).wait_send()


def side_sems():
    return [DMA((2, 3)), DMA((2, 3)), DMA((NX, 2)), DMA((NX, 2))]


def layer_kernel(
    n, heads_win, tok, gain, kd, vd, qd, qwd, kvw, pd, pw, lam, sink, ogain, out,
    w1, w2, raw, nbuf, acc1, acc2, kbuf, pdb, pwb, q, qw, kw, top, tot, acc, y, yd, yv, give, take, sums, facc,
    lsem, z1s, z1r, y1s, y1r, z2s, z2r, y2s, y2r, zks, zkr, hs, hr, us, ur, ts, tr, ws, wr, *sems,
):
    me, x, c = (lax.axis_index(a) for a in ("sp", "tp_0", "tp_1"))
    t = 2 * x + c
    block = raw.shape[1]
    rows = 2 * NX * block
    depth = w1.shape[1]
    part = kvw.shape[2] // 2
    head = t * heads_win // (WIN_HEADS // KV_HEADS)
    wq = qwd.shape[1]
    local = []
    at = 0
    for w in (kd, vd, qd):
        local.append((w, w1.at[me, :, pl.ds(at, w.shape[1])]))
        at += w.shape[1]
    local += [
        (qwd, w2.at[me, :, pl.ds(0, wq)]),
        (kvw.at[head, :, pl.ds(pl.multiple_of(c * part, part), part)], w2.at[me, :, pl.ds(wq, part)]),
        (tok, raw.at[t]),
        (pd, pdb.at[t]),
        (pw, pwb),
    ]
    local = [pltpu.make_async_copy(a, b, lsem.at[i]) for i, (a, b) in enumerate(local)]
    for copy in local:
        copy.start()

    swap1 = Swap(n, w1, CUT, y1s, y1r)
    swap2 = Swap(n, w2, depth // 2, y2s, y2r)
    ring1 = Ring(n, w1, swap1.base, (48, 48, 48, swap1.kept - 144), z1s, z1r)
    ring2 = Ring(n, w2, swap2.base, (depth // 4,) * 2, z2s, z2r)
    ring = Ring(n, kbuf, 0, (rows // 4,) * 4, zks, zkr)
    side = Side(None, raw, block // 2, *sems[:4])
    late = Side(None, pdb, depth // 2, *sems[4:])

    def peer(k):
        return {"tp_0": lax.rem(x + k // 2, NX), "tp_1": lax.rem(c + k % 2, 2)}

    greet([ring.to[0], ring.to[1], swap1.to] + [peer(k) for k in range(1, 2 * NX)])

    for copy in local[:3]:
        copy.wait()
    for k in range(4):
        ring1.start(0, k)
    local[5].wait()
    side.start()
    acc1[...] = jnp.zeros_like(acc1)
    acc2[...] = jnp.zeros_like(acc2)
    top[...] = jnp.full_like(top, -jnp.inf)
    tot[...] = jnp.zeros_like(tot)
    acc[...] = jnp.zeros_like(acc)
    for copy in local[3:5] + local[6:]:
        copy.wait()

    def normalise(quarter):
        tile = 32
        per = raw.shape[0] * block // tile // 4

        def one(j, carry):
            i = quarter * per + j
            slot, r = i // (block // tile), lax.rem(i, block // tile)
            v = raw[slot, pl.ds(pl.multiple_of(r * tile, tile), tile), :].astype(F32)
            v = v * lax.rsqrt(jnp.mean(v * v, axis=-1, keepdims=True) + EPS) * gain[...]
            v = v.astype(BF16)
            for o in range(n):
                nbuf[o, pl.ds(pl.multiple_of(i * tile, tile), tile), :] = v[:, o * depth : (o + 1) * depth]
            return carry

        lax.fori_loop(0, per, one, 0)

    def gather(w, swap, total, lo, hi):
        def one(j, carry):
            o = lax.rem(me + jnp.where(lax.rem(j, 2) == 1, (j + 1) // 2, n - j // 2), n)

            @pl.when(j > 0)
            def _():
                swap.land(o)

            total[...] += jnp.dot(nbuf[o], w[o], preferred_element_type=F32)
            return carry

        lax.fori_loop(lo, hi, one, 0)

    last = n // 2 - 1

    def swap_both(swap, ring_, hops):
        for d in (0, 1):
            swap.start(ring_.origin(d, hops))

    def hop2(s, k):
        ring2.land(s, k)
        ring2.start(s + 1, k)
        if k == 1:
            swap_both(swap2, ring2, s + 1)

    def phase1(s, carry):
        for k in range(4):
            ring1.land(s, k)
            ring1.start(s + 1, k)
            if k == 0:
                for i in range(3):

                    @pl.when(s == i + 1)
                    def _():
                        side.step(i)

                @pl.when(s == last - 3)
                def _():
                    side.finish()
                    late.start()

            @pl.when(s == last - 3)
            def _():
                normalise(k)

            @pl.when(s == last - 2)
            def _():
                gather(w1, swap1, acc1, 3 * k, min(3 * k + 3, 2 * last - 3))

            if k % 2 == 1:

                @pl.when(s >= 2)
                def _():
                    hop2(s - 2, k // 2)

        swap_both(swap1, ring1, s + 1)

        @pl.when(s == 1)
        def _():
            for k in (0, 1):
                ring2.start(0, k)

        return carry

    lax.fori_loop(0, last - 1, phase1, 0)
    done = 2 * last - 3
    for k in range(4):
        ring1.land(last - 1, k)
        if k < 2:
            ring1.start(last, k)
        if k % 2 == 0:
            gather(w1, swap1, acc1, done + k // 2, done + k // 2 + 1)
        else:
            hop2(last - 3, k // 2)
    swap_both(swap1, ring1, last)
    for k in (0, 1):
        ring1.land(last, k)
    swap1.start(ring1.origin(0, last + 1))
    late.step(0)
    for k in (0, 1):
        hop2(last - 2, k)
    gather(w1, swap1, acc1, done + 2, done + 4)
    ring2.land(last - 1, 0)
    ring2.start(last, 0)
    ring2.land(last - 1, 1)
    swap_both(swap2, ring2, last)
    gather(w1, swap1, acc1, n - 1, n)
    kvd = kbuf.shape[2]
    kbuf[me] = acc1[:, :kvd].astype(BF16)
    q[...] = acc1[:, kvd:].astype(BF16)
    for k in range(4):
        ring.start(0, k)

    def edge(d, inward):
        src = pl.ds(rows, WINDOW) if d == 0 else pl.ds(WINDOW, WINDOW)
        dst = pl.ds(0, WINDOW) if d == 0 else pl.ds(rows + WINDOW, WINDOW)
        target = kw.at[c, dst]
        return remote(target if inward else kw.at[c, src], target, hs.at[d], hr.at[d], ring.to[d])

    spans = (pl.ds(WINDOW, rows), pl.ds(0, WINDOW), pl.ds(rows + WINDOW, WINDOW))

    def twin(i, inward):
        ref = kw.at[1 - c if inward else c, spans[i]]
        return remote(ref, ref, us.at[i], ur.at[i], side.other)

    def trade(k, inward):
        if inward:
            ref = yd.at[2 * lax.rem(x + NX - k // 2, NX) + lax.rem(c + k % 2, 2)]
            return remote(ref, ref, ts.at[k], tr.at[k], peer(k))
        src = y.at[2 * lax.rem(x + k // 2, NX) + lax.rem(c + k % 2, 2)]
        return remote(src, yd.at[t], ts.at[k], tr.at[k], peer(k))

    pass_on = remote(give, take, ws.at[0], wr.at[0], side.other)

    def deal(k, inward):
        to = lax.rem(x + k, NX)
        return remote(sums.at[k - 1] if inward else take.at[to], sums.at[k - 1], ws.at[k], wr.at[k], {"tp_0": to})

    scale = HEAD**-0.5
    lanes = HEAD
    contract_last = (((1,), (1,)), ((), ()))

    def attend(o):
        def one(m, carry):
            cols = pl.ds(pl.multiple_of(m * HEAD, HEAD), HEAD)
            s = lax.dot_general(q[:, cols], kbuf[o, :, cols], contract_last, preferred_element_type=F32)
            s = s * (scale * LOG2E)
            reps = s.shape[1] // lanes
            was = top[m]
            now = jnp.maximum(was, jnp.max(s, axis=1, keepdims=True))
            fade = jnp.exp2(was - now)
            e = jnp.exp2(s - jnp.concatenate([now] * reps, axis=1))
            some = e[:, :lanes]
            for j in range(1, reps):
                some = some + e[:, j * lanes : (j + 1) * lanes]
            tot[m] = tot[m] * fade + some
            top[m] = now
            acc[m] = acc[m] * jnp.concatenate([fade] * (VDIM // lanes), axis=1) + jnp.dot(
                e.astype(BF16), kbuf[o, :, 2 * HEAD :], preferred_element_type=F32
            )
            return carry

        for m in range(2):
            one(m, 0)

    def window(lo, hi):
        span = 3 * WINDOW
        heads = wq // HEAD
        i_q = lax.broadcasted_iota(jnp.int32, (WINDOW, span), 0)
        i_k = lax.broadcasted_iota(jnp.int32, (WINDOW, span), 1)
        near = jnp.abs(i_k - WINDOW - i_q) <= WINDOW

        def one(b, carry):
            r = pl.ds(pl.multiple_of(b * WINDOW, WINDOW), WINDOW)
            band = pl.ds(pl.multiple_of(b * WINDOW, WINDOW), span)
            where = i_k + (me * rows + b * WINDOW - WINDOW)
            valid = near & (where >= 0) & (where < n * rows)
            for h in range(heads):
                cols = pl.ds(h * HEAD, HEAD)
                s = lax.dot_general(qw[r, cols], kw[0, band, :], contract_last, preferred_element_type=F32)
                s = jnp.where(valid, s * scale, -jnp.inf)
                sunk = jnp.full((WINDOW, lanes), sink[h], F32)
                peak = jnp.maximum(jnp.max(s, axis=1, keepdims=True), sunk)
                e = jnp.exp(s - jnp.concatenate([peak] * 3, axis=1))
                whole = jnp.sum(e, axis=1, keepdims=True) + jnp.exp(sunk - peak)
                w = (e / jnp.concatenate([whole] * 3, axis=1)).astype(BF16)
                res = jnp.dot(w, kw[1, band, :], preferred_element_type=F32).astype(BF16)
                for j in range(WINDOW // block):
                    yv[j % 2, b * (WINDOW // block // 2) + j // 2, :, cols] = res[j * block : (j + 1) * block]
            return carry

        lax.fori_loop(lo, hi, one, 0)

    width = 512

    def columns(one):
        def run(j, carry):
            one(pl.ds(pl.multiple_of(j * width, width), width))
            return carry

        lax.fori_loop(0, out.shape[1] // width, run, 0)

    def window_rows(core, cols):
        ys = yv[core].reshape(NX * block, wq)
        return jnp.dot(ys, pwb[:, cols], preferred_element_type=F32).reshape(NX, block, width)

    def to_give(cols):
        give[:, :, cols] = window_rows(1 - c, cols).astype(BF16)

    def to_sum(cols):
        take[:, :, cols] = (window_rows(c, cols) + take[:, :, cols].astype(F32)).astype(BF16)

    attend(me)

    def phase2(s, carry):
        for k in range(4):
            ring.land(s, k)
            ring.start(s + 1, k)
            if k == 0:

                @pl.when(s == 0)
                def _():
                    ring2.land(last, 0)
                    swap2.start(ring2.origin(0, last + 1))

                @pl.when(s == 1)
                def _():
                    gather(w2, swap2, acc2, 0, n // 2)

                @pl.when(s == 2)
                def _():
                    for d in (0, 1):
                        edge(d, True).wait_recv()
                        twin(d + 1, False).start()
                    late.step(2)

                @pl.when(s == 3)
                def _():
                    window(rows // WINDOW // 2, rows // WINDOW)

                @pl.when(s == 4)
                def _():
                    pass_on.wait_recv()
                    columns(to_sum)
                    for i in range(1, NX):
                        deal(i, False).start()

            if k == 2:

                @pl.when(s == 0)
                def _():
                    late.step(1)

                @pl.when(s == 1)
                def _():
                    gather(w2, swap2, acc2, n // 2, n)
                    kw[c, spans[0]] = acc2[:, wq:].astype(BF16)
                    qw[...] = acc2[:, :wq].astype(BF16)
                    for d in (0, 1):
                        edge(d, False).start()
                    twin(0, False).start()

                @pl.when(s == 2)
                def _():
                    for i in range(3):
                        twin(i, True).wait_recv()
                    window(0, rows // WINDOW // 2)

                @pl.when(s == 3)
                def _():
                    columns(to_give)
                    pass_on.start()

            if k % 2 == 1:

                @pl.when(s > 0)
                def _():
                    attend(ring.origin(k // 2, s))

        return carry

    lax.fori_loop(0, last - 1, phase2, 0)
    for k in range(4):
        ring.land(last - 1, k)
        if k < 2:
            ring.start(last, k)
        if k % 2 == 1:
            attend(ring.origin(k // 2, last - 1))
    late.finish()
    for k in range(1, NX):
        deal(k, True).wait_recv()
    facc[...] = take[x].astype(F32)
    for k in range(1, NX):
        facc[...] += sums[k - 1].astype(F32)

    def both(i, carry):
        attend(lax.rem(me + n - last + 2 * last * i, n))
        return carry

    lax.fori_loop(0, 2, both, 0)
    for k in (0, 1):
        ring.land(last, k)
    attend(lax.rem(me + last + 1, n))

    def close(j, carry):
        r = pl.ds(pl.multiple_of(j * block, block), block)
        maps = [acc[m, r, :] / jnp.sum(tot[m, r, :], axis=1, keepdims=True) for m in range(2)]
        d = maps[0] - lam[0] * maps[1]
        d = d * lax.rsqrt(jnp.mean(d * d, axis=-1, keepdims=True) + EPS) * ogain[...]
        y[j] = d.astype(BF16)
        return carry

    lax.fori_loop(0, 2 * NX, close, 0)
    for k in (4, 5, 2, 3, 6, 7, 1):
        trade(k, False).start()
    yd[t] = y[t]
    wide = 1024
    for i, away in enumerate((0, 1, 3, 2)):
        for k in (2 * away, 2 * away + 1):
            if k > 0:
                trade(k, True).wait_recv()
        first = 2 * lax.rem(x + NX - away, NX)

        def add(j, carry):
            cols = pl.ds(pl.multiple_of(j * wide, wide), wide)
            total = facc[:, cols]
            for h in (0, 1):
                total = total + jnp.dot(yd[first + h], pdb[first + h, :, cols], preferred_element_type=F32)
            if i == NX - 1:
                out[:, cols] = total.astype(out.dtype)
            else:
                facc[:, cols] = total
            return carry

        lax.fori_loop(0, out.shape[1] // wide, add, 0)
    for k in range(1, 2 * NX):
        trade(k, False).wait_send()
    for d in (0, 1):
        edge(d, False).wait_send()
    for i in range(3):
        twin(i, False).wait_send()
    pass_on.wait_send()
    for k in range(1, NX):
        deal(k, False).wait_send()
    for r in (ring1, ring2, ring, swap1, swap2, side, late):
        r.drain()


def body(
    n, tokens, norm_gain, query_diff, key_diff, value_diff, lam, output_norm_gain,
    query_win, keyval_win, sink, proj_diff, proj_win,
):
    block, model = tokens.shape
    rows = block * 2 * NX
    depth, wq = query_win.shape
    kvd = key_diff.shape[1] + value_diff.shape[1]
    dq = query_diff.shape[1]
    part = keyval_win.shape[2] // 2
    hops = n // 2

    def pair(*shape):
        return [DMA(shape), DMA(shape)]

    return pl.pallas_call(
        functools.partial(layer_kernel, n, sink.shape[0]),
        out_shape=jax.ShapeDtypeStruct((block, model), BF16),
        in_specs=[
            pl.BlockSpec(memory_space=m)
            for m in [ANY, VMEM] + [ANY] * 7 + [pltpu.SMEM, pltpu.SMEM, VMEM]
        ],
        out_specs=pl.BlockSpec(memory_space=VMEM),
        scratch_shapes=[
            VMEM((n, depth, kvd + dq), BF16),
            VMEM((n, depth, wq + part), BF16),
            VMEM((2 * NX, block, model), BF16),
            VMEM((n, rows, depth), BF16),
            VMEM((rows, kvd + dq), F32),
            VMEM((rows, wq + part), F32),
            VMEM((n, rows, kvd), BF16),
            VMEM((2 * NX,) + proj_diff.shape, BF16),
            VMEM(proj_win.shape, BF16),
            VMEM((rows, dq), BF16),
            VMEM((rows, wq), BF16),
            VMEM((2, rows + 2 * WINDOW, part), BF16),
            VMEM((2, rows, HEAD), F32),
            VMEM((2, rows, HEAD), F32),
            VMEM((2, rows, VDIM), F32),
            VMEM((2 * NX, block, VDIM), BF16),
            VMEM((2 * NX, block, VDIM), BF16),
            VMEM((2, NX, block, wq), BF16),
            VMEM((NX, block, model), BF16),
            VMEM((NX, block, model), BF16),
            VMEM((NX - 1, block, model), BF16),
            VMEM((block, model), F32),
            DMA((8,)),
        ]
        + pair(2, hops, 4)
        + pair(n)
        + pair(2, hops, 2)
        + pair(n)
        + pair(2, hops, 4)
        + pair(2)
        + pair(3)
        + pair(2 * NX)
        + pair(NX)
        + side_sems()
        + side_sems(),
        compiler_params=pltpu.CompilerParams(
            collective_id=0, has_side_effects=True, vmem_limit_bytes=67_000_000
        ),
    )(
        tokens, norm_gain.reshape(1, model), key_diff, value_diff, query_diff, query_win, keyval_win,
        proj_diff, proj_win, lam, sink, output_norm_gain.reshape(1, VDIM),
    )


def solution(mesh):
    torus = Mesh(
        mesh.devices.reshape(mesh.shape["grp"], mesh.shape["sp"], NX, 2),
        ("grp", "sp", "tp_0", "tp_1"),
    )
    return jax.shard_map(
        functools.partial(body, mesh.shape["sp"]),
        mesh=torus,
        in_specs=(
            P(GRP_SP_TP, None),
            P(),
            P("sp", TP),
            P("sp", TP),
            P("sp", TP),
            P(TP),
            P(),
            P("sp", TP),
            P(None, "sp", None),
            P(TP),
            P(TP, None),
            P(TP, None),
        ),
        out_specs=P(GRP_SP_TP, None),
        check_vma=False,
    )
```

time: 223 us -> 207 us (0.928)
  Pallas kernels: 218 us -> 205 us
    pallas_call x2 -> x1, Pallas kernels: 218 us -> 205 us  [body(): pl.pallas_call(functools.partial(layer_kernel, n, sink.shape[0]), out_sha...]
where the time goes in v3:
time: 207 us
  Pallas kernels  205 us (99%)
    pallas_call x1, Pallas kernels, body(): pl.pallas_call(functools.partial(layer_kernel, n, sink.shape[0]), out_sha...  205 us

profile of v3, /device:TPU:33, one launch (start us, length us, event | category | flops | bytes accessed | tf_op | source)
XLA Modules:
  0.0 207.1 jit_solution(1471680996405976896)
XLA Ops:
  0.7 204.6 %shard_map.118 = bf16[64,4096]{1,0:T(8,128)(2,1)} custom-call(bf16[64,4096]{1,0:T(8,128)(2,1)} %tok.1, f32[1,4096]{1,0:T(1,128)} %bitcast.2, bf16[256,256]{1,0:T(8,128)(2,1)} %kd.1, bf16[256,256]{1,0:T(8,128)(2,1)} %vd.1, bf16[256,256]{1,0:T(8,128)(2,1)} %qd.1, bf16[256,256]{1,0:T(8,128)(2,1)} %qwd.1, bf16[4,256,256]{2,1,0:T(8,128)(2,1)} %kvw.1, ...), custom_call_target="tpu_custom_call" | custom-call | tf_op jit(solution)/shard_map/pallas_call | solution.py:610
  205.2 1.9 copy.15

commit v4 on v3

--- a/solution.py
+++ b/solution.py
@@ -286,8 +286,13 @@
     def hop2(s, k):
         ring2.land(s, k)
         ring2.start(s + 1, k)
-        if k == 1:
-            swap_both(swap2, ring2, s + 1)
+
+    def late_swaps(lo, hi):
+        def one(h, carry):
+            swap_both(swap2, ring2, h)
+            return carry
+
+        lax.fori_loop(lo, hi, one, 0)
 
     def phase1(s, carry):
         for k in range(4):
@@ -299,11 +304,12 @@
                     @pl.when(s == i + 1)
                     def _():
                         side.step(i)
+                        if i == 2:
+                            late.start()
 
                 @pl.when(s == last - 3)
                 def _():
                     side.finish()
-                    late.start()
 
             @pl.when(s == last - 3)
             def _():
@@ -334,17 +340,18 @@
         ring1.land(last - 1, k)
         if k < 2:
             ring1.start(last, k)
-        if k % 2 == 0:
-            gather(w1, swap1, acc1, done + k // 2, done + k // 2 + 1)
-        else:
+        if k % 2 == 1:
             hop2(last - 3, k // 2)
+        if k == 2:
+            gather(w1, swap1, acc1, done, done + 1)
     swap_both(swap1, ring1, last)
+    gather(w1, swap1, acc1, done + 1, done + 2)
     for k in (0, 1):
         ring1.land(last, k)
     swap1.start(ring1.origin(0, last + 1))
-    late.step(0)
     for k in (0, 1):
         hop2(last - 2, k)
+    late_swaps(1, last)
     gather(w1, swap1, acc1, done + 2, done + 4)
     ring2.land(last - 1, 0)
     ring2.start(last, 0)
@@ -468,36 +475,13 @@
                 def _():
                     ring2.land(last, 0)
                     swap2.start(ring2.origin(0, last + 1))
+                    late.step(0)
 
                 @pl.when(s == 1)
                 def _():
-                    gather(w2, swap2, acc2, 0, n // 2)
-
-                @pl.when(s == 2)
-                def _():
-                    for d in (0, 1):
-                        edge(d, True).wait_recv()
-                        twin(d + 1, False).start()
-                    late.step(2)
+                    late.step(1)
 
                 @pl.when(s == 3)
-                def _():
-                    window(rows // WINDOW // 2, rows // WINDOW)
-
-                @pl.when(s == 4)
-                def _():
-                    pass_on.wait_recv()
-                    columns(to_sum)
-                    for i in range(1, NX):
-                        deal(i, False).start()
-
-            if k == 2:
-
-                @pl.when(s == 0)
-                def _():
-                    late.step(1)
-
-                @pl.when(s == 1)
                 def _():
                     gather(w2, swap2, acc2, n // 2, n)
                     kw[c, spans[0]] = acc2[:, wq:].astype(BF16)
@@ -506,16 +490,40 @@
                         edge(d, False).start()
                     twin(0, False).start()
 
-                @pl.when(s == 2)
+                @pl.when(s == 4)
                 def _():
                     for i in range(3):
                         twin(i, True).wait_recv()
                     window(0, rows // WINDOW // 2)
 
-                @pl.when(s == 3)
+                @pl.when(s == 5)
                 def _():
                     columns(to_give)
                     pass_on.start()
+
+            if k == 2:
+
+                @pl.when(s == 2)
+                def _():
+                    gather(w2, swap2, acc2, 0, n // 2)
+
+                @pl.when(s == 3)
+                def _():
+                    for d in (0, 1):
+                        edge(d, True).wait_recv()
+                        twin(d + 1, False).start()
+                    late.step(2)
+
+                @pl.when(s == 4)
+                def _():
+                    window(rows // WINDOW // 2, rows // WINDOW)
+
+                @pl.when(s == 5)
+                def _():
+                    pass_on.wait_recv()
+                    columns(to_sum)
+                    for i in (2, 1, 3):
+                        deal(i, False).start()
 
             if k % 2 == 1:
 
@@ -533,63 +541,71 @@
         if k % 2 == 1:
             attend(ring.origin(k // 2, last - 1))
     late.finish()
-    for k in range(1, NX):
-        deal(k, True).wait_recv()
-    facc[...] = take[x].astype(F32)
-    for k in range(1, NX):
-        facc[...] += sums[k - 1].astype(F32)
-
-    def both(i, carry):
-        attend(lax.rem(me + n - last + 2 * last * i, n))
-        return carry
-
-    lax.fori_loop(0, 2, both, 0)
-    for k in (0, 1):
-        ring.land(last, k)
-    attend(lax.rem(me + last + 1, n))
-
-    def close(j, carry):
-        r = pl.ds(pl.multiple_of(j * block, block), block)
-        maps = [acc[m, r, :] / jnp.sum(tot[m, r, :], axis=1, keepdims=True) for m in range(2)]
-        d = maps[0] - lam[0] * maps[1]
-        d = d * lax.rsqrt(jnp.mean(d * d, axis=-1, keepdims=True) + EPS) * ogain[...]
-        y[j] = d.astype(BF16)
-        return carry
-
-    lax.fori_loop(0, 2 * NX, close, 0)
-    for k in (4, 5, 2, 3, 6, 7, 1):
-        trade(k, False).start()
-    yd[t] = y[t]
-    wide = 1024
-    for i, away in enumerate((0, 1, 3, 2)):
-        for k in (2 * away, 2 * away + 1):
-            if k > 0:
-                trade(k, True).wait_recv()
-        first = 2 * lax.rem(x + NX - away, NX)
-
-        def add(j, carry):
-            cols = pl.ds(pl.multiple_of(j * wide, wide), wide)
-            total = facc[:, cols]
-            for h in (0, 1):
-                total = total + jnp.dot(yd[first + h], pdb[first + h, :, cols], preferred_element_type=F32)
-            if i == NX - 1:
-                out[:, cols] = total.astype(out.dtype)
-            else:
-                facc[:, cols] = total
-            return carry
-
-        lax.fori_loop(0, out.shape[1] // wide, add, 0)
-    for k in range(1, 2 * NX):
-        trade(k, False).wait_send()
+    for r in (ring1, ring2, swap1, swap2, side, late):
+        r.drain()
     for d in (0, 1):
         edge(d, False).wait_send()
     for i in range(3):
         twin(i, False).wait_send()
     pass_on.wait_send()
+
+    def both(i, carry):
+        attend(lax.rem(me + n - last + 2 * last * i, n))
+        return carry
+
+    lax.fori_loop(0, 2, both, 0)
+    for k in (0, 1):
+        ring.land(last, k)
+    attend(lax.rem(me + last + 1, n))
+
+    def close(j):
+        r = pl.ds(pl.multiple_of(j * block, block), block)
+        parts = [1.0 / jnp.sum(tot[m, r, :], axis=1, keepdims=True) for m in range(2)]
+        d = acc[0, r, :] * parts[0] - acc[1, r, :] * (lam[0] * parts[1])
+        d = d * lax.rsqrt(jnp.mean(d * d, axis=-1, keepdims=True) + EPS) * ogain[...]
+        return d.astype(BF16)
+
+    for k in (4, 5, 2, 6, 3, 7, 1):
+        j = 2 * lax.rem(x + k // 2, NX) + lax.rem(c + k % 2, 2)
+        y[j] = close(j)
+        trade(k, False).start()
+    yd[t] = close(t)
+    wide = 1024
+
+    def add(total, away, cols):
+        first = 2 * lax.rem(x + NX - away, NX)
+        for h in (0, 1):
+            total = total + jnp.dot(yd[first + h], pdb[first + h, :, cols], preferred_element_type=F32)
+        return total
+
+    def begin(j, carry):
+        cols = pl.ds(pl.multiple_of(j * wide, wide), wide)
+        total = take[x, :, cols].astype(F32)
+        for k in range(1, NX):
+            total = total + sums[k - 1, :, cols].astype(F32)
+        facc[:, cols] = add(total, 0, cols)
+        return carry
+
+    def finish(j, carry):
+        cols = pl.ds(pl.multiple_of(j * wide, wide), wide)
+        total = facc[:, cols]
+        for away in (1, 3, 2):
+            total = add(total, away, cols)
+        out[:, cols] = total.astype(out.dtype)
+        return carry
+
+    for k in range(1, NX):
+        deal(k, True).wait_recv()
+    trade(1, True).wait_recv()
+    lax.fori_loop(0, out.shape[1] // wide, begin, 0)
+    for k in range(2, 2 * NX):
+        trade(k, True).wait_recv()
+    lax.fori_loop(0, out.shape[1] // wide, finish, 0)
+    for k in range(1, 2 * NX):
+        trade(k, False).wait_send()
     for k in range(1, NX):
         deal(k, False).wait_send()
-    for r in (ring1, ring2, ring, swap1, swap2, side, late):
-        r.drain()
+    ring.drain()
 
 
 def body(

time: 207 us -> 198 us (0.957)
  Pallas kernels: 205 us -> 194 us
    pallas_call x1, Pallas kernels: 205 us -> 194 us  [body(): pl.pallas_call(functools.partial(layer_kernel, n, sink.shape[0]), out_sha...]
where the time goes in v4:
time: 198 us; the launch traced here: 197 us
  Pallas kernels  194 us (98%)
    pallas_call x1, Pallas kernels, body(): pl.pallas_call(functools.partial(layer_kernel, n, sink.shape[0]), out_sha...  194 us

profile of v4, /device:TPU:33, one launch (start us, length us, event | category | flops | bytes accessed | tf_op | source)
XLA Modules:
  0.0 197.0 jit_solution(8334298046406766674)
XLA Ops:
  0.7 194.4 %shard_map.118 = bf16[64,4096]{1,0:T(8,128)(2,1)} custom-call(bf16[64,4096]{1,0:T(8,128)(2,1)} %tok.1, f32[1,4096]{1,0:T(1,128)} %bitcast.2, bf16[256,256]{1,0:T(8,128)(2,1)} %kd.1, bf16[256,256]{1,0:T(8,128)(2,1)} %vd.1, bf16[256,256]{1,0:T(8,128)(2,1)} %qd.1, bf16[256,256]{1,0:T(8,128)(2,1)} %qwd.1, bf16[4,256,256]{2,1,0:T(8,128)(2,1)} %kvw.1, ...), custom_call_target="tpu_custom_call" | custom-call | tf_op jit(solution)/shard_map/pallas_call | solution.py:626
  195.1 1.9 copy.15

commit v5 on v4

--- a/solution.py
+++ b/solution.py
@@ -14,7 +14,7 @@
 WINDOW = 128
 VDIM = 256
 NX = 4
-CUT = 80
+CUT = 96
 TP = ("tp_0", "tp_1")
 GRP_SP_TP = ("grp", "sp", "tp_0", "tp_1")
 EPS = 1e-06
@@ -194,7 +194,7 @@
 
 def layer_kernel(
     n, heads_win, tok, gain, kd, vd, qd, qwd, kvw, pd, pw, lam, sink, ogain, out,
-    w1, w2, raw, nbuf, acc1, acc2, kbuf, pdb, pwb, q, qw, kw, top, tot, acc, y, yd, yv, give, take, sums, facc,
+    w1, w2, raw, nbuf, acc1, acc2, kbuf, pdb, pwb, q, qw, kw, top, tot, acc, y, yd, yv, give, take, far, sums, facc,
     lsem, z1s, z1r, y1s, y1r, z2s, z2r, y2s, y2r, zks, zkr, hs, hr, us, ur, ts, tr, ws, wr, *sems,
 ):
     me, x, c = (lax.axis_index(a) for a in ("sp", "tp_0", "tp_1"))
@@ -223,7 +223,7 @@
 
     swap1 = Swap(n, w1, CUT, y1s, y1r)
     swap2 = Swap(n, w2, depth // 2, y2s, y2r)
-    ring1 = Ring(n, w1, swap1.base, (48, 48, 48, swap1.kept - 144), z1s, z1r)
+    ring1 = Ring(n, w1, swap1.base, (48, 32, 32, swap1.kept - 112), z1s, z1r)
     ring2 = Ring(n, w2, swap2.base, (depth // 4,) * 2, z2s, z2r)
     ring = Ring(n, kbuf, 0, (rows // 4,) * 4, zks, zkr)
     side = Side(None, raw, block // 2, *sems[:4])
@@ -327,7 +327,7 @@
 
         swap_both(swap1, ring1, s + 1)
 
-        @pl.when(s == 1)
+        @pl.when(s == 0)
         def _():
             for k in (0, 1):
                 ring2.start(0, k)
@@ -385,9 +385,22 @@
 
     pass_on = remote(give, take, ws.at[0], wr.at[0], side.other)
 
-    def deal(k, inward):
-        to = lax.rem(x + k, NX)
-        return remote(sums.at[k - 1] if inward else take.at[to], sums.at[k - 1], ws.at[k], wr.at[k], {"tp_0": to})
+    def relay(d, inward):
+        src = far.at[d] if inward else take.at[lax.rem(x + 2, NX), pl.ds(d * (block // 2), block // 2)]
+        return remote(src, far.at[d], ws.at[1 + d], wr.at[1 + d], side.to[d])
+
+    def deal(d, inward):
+        src = sums.at[d] if inward else take.at[lax.rem(x + (1, NX - 1)[d], NX)]
+        return remote(src, sums.at[d], ws.at[3 + d], wr.at[3 + d], side.to[d])
+
+    def merge():
+        for d in (0, 1):
+            relay(d, True).wait_recv()
+            to = lax.rem(x + (1, NX - 1)[d], NX)
+            half = pl.ds(d * (block // 2), block // 2)
+            take[to, half, :] = (take[to, half, :].astype(F32) + far[d].astype(F32)).astype(BF16)
+        for d in (0, 1):
+            deal(d, False).start()
 
     scale = HEAD**-0.5
     lanes = HEAD
@@ -416,14 +429,15 @@
         for m in range(2):
             one(m, 0)
 
-    def window(lo, hi):
+    def window(lo, hi, stride):
         span = 3 * WINDOW
         heads = wq // HEAD
         i_q = lax.broadcasted_iota(jnp.int32, (WINDOW, span), 0)
         i_k = lax.broadcasted_iota(jnp.int32, (WINDOW, span), 1)
         near = jnp.abs(i_k - WINDOW - i_q) <= WINDOW
 
-        def one(b, carry):
+        def one(i, carry):
+            b = i * stride
             r = pl.ds(pl.multiple_of(b * WINDOW, WINDOW), WINDOW)
             band = pl.ds(pl.multiple_of(b * WINDOW, WINDOW), span)
             where = i_k + (me * rows + b * WINDOW - WINDOW)
@@ -481,7 +495,31 @@
                 def _():
                     late.step(1)
 
+                @pl.when(s == 2)
+                def _():
+                    gather(w2, swap2, acc2, 0, n // 2)
+
                 @pl.when(s == 3)
+                def _():
+                    twin(0, True).wait_recv()
+                    window(1, rows // WINDOW - 1, 1)
+
+                @pl.when(s == 4)
+                def _():
+                    for i in (1, 2):
+                        twin(i, True).wait_recv()
+                    window(0, 2, rows // WINDOW - 1)
+
+                @pl.when(s == 5)
+                def _():
+                    pass_on.wait_recv()
+                    columns(to_sum)
+                    for d in (0, 1):
+                        relay(d, False).start()
+
+            if k == 2:
+
+                @pl.when(s == 2)
                 def _():
                     gather(w2, swap2, acc2, n // 2, n)
                     kw[c, spans[0]] = acc2[:, wq:].astype(BF16)
@@ -490,23 +528,6 @@
                         edge(d, False).start()
                     twin(0, False).start()
 
-                @pl.when(s == 4)
-                def _():
-                    for i in range(3):
-                        twin(i, True).wait_recv()
-                    window(0, rows // WINDOW // 2)
-
-                @pl.when(s == 5)
-                def _():
-                    columns(to_give)
-                    pass_on.start()
-
-            if k == 2:
-
-                @pl.when(s == 2)
-                def _():
-                    gather(w2, swap2, acc2, 0, n // 2)
-
                 @pl.when(s == 3)
                 def _():
                     for d in (0, 1):
@@ -516,14 +537,8 @@
 
                 @pl.when(s == 4)
                 def _():
-                    window(rows // WINDOW // 2, rows // WINDOW)
-
-                @pl.when(s == 5)
-                def _():
-                    pass_on.wait_recv()
-                    columns(to_sum)
-                    for i in (2, 1, 3):
-                        deal(i, False).start()
+                    columns(to_give)
+                    pass_on.start()
 
             if k % 2 == 1:
 
@@ -538,6 +553,8 @@
         ring.land(last - 1, k)
         if k < 2:
             ring.start(last, k)
+        if k == 0:
+            merge()
         if k % 2 == 1:
             attend(ring.origin(k // 2, last - 1))
     late.finish()
@@ -581,8 +598,8 @@
     def begin(j, carry):
         cols = pl.ds(pl.multiple_of(j * wide, wide), wide)
         total = take[x, :, cols].astype(F32)
-        for k in range(1, NX):
-            total = total + sums[k - 1, :, cols].astype(F32)
+        for d in (0, 1):
+            total = total + sums[d, :, cols].astype(F32)
         facc[:, cols] = add(total, 0, cols)
         return carry
 
@@ -594,8 +611,8 @@
         out[:, cols] = total.astype(out.dtype)
         return carry
 
-    for k in range(1, NX):
-        deal(k, True).wait_recv()
+    for d in (0, 1):
+        deal(d, True).wait_recv()
     trade(1, True).wait_recv()
     lax.fori_loop(0, out.shape[1] // wide, begin, 0)
     for k in range(2, 2 * NX):
@@ -603,8 +620,9 @@
     lax.fori_loop(0, out.shape[1] // wide, finish, 0)
     for k in range(1, 2 * NX):
         trade(k, False).wait_send()
-    for k in range(1, NX):
-        deal(k, False).wait_send()
+    for d in (0, 1):
+        relay(d, False).wait_send()
+        deal(d, False).wait_send()
     ring.drain()
 
 
@@ -652,7 +670,8 @@
             VMEM((2, NX, block, wq), BF16),
             VMEM((NX, block, model), BF16),
             VMEM((NX, block, model), BF16),
-            VMEM((NX - 1, block, model), BF16),
+            VMEM((2, block // 2, model), BF16),
+            VMEM((2, block, model), BF16),
             VMEM((block, model), F32),
             DMA((8,)),
         ]
@@ -664,7 +683,7 @@
         + pair(2)
         + pair(3)
         + pair(2 * NX)
-        + pair(NX)
+        + pair(5)
         + side_sems()
         + side_sems(),
         compiler_params=pltpu.CompilerParams(

time: 198 us -> 189 us (0.955)
  Pallas kernels: 194 us -> 186 us
    pallas_call x1, Pallas kernels: 194 us -> 186 us  [body(): pl.pallas_call(functools.partial(layer_kernel, n, sink.shape[0]), out_sha...]
where the time goes in v5:
time: 189 us
  Pallas kernels  186 us (98%)
    pallas_call x1, Pallas kernels, body(): pl.pallas_call(functools.partial(layer_kernel, n, sink.shape[0]), out_sha...  186 us

profile of v5, /device:TPU:33, one launch (start us, length us, event | category | flops | bytes accessed | tf_op | source)
XLA Modules:
  0.0 189.0 jit_solution(13149012305821845388)
XLA Ops:
  0.7 186.4 %shard_map.118 = bf16[64,4096]{1,0:T(8,128)(2,1)} custom-call(bf16[64,4096]{1,0:T(8,128)(2,1)} %tok.1, f32[1,4096]{1,0:T(1,128)} %bitcast.2, bf16[256,256]{1,0:T(8,128)(2,1)} %kd.1, bf16[256,256]{1,0:T(8,128)(2,1)} %vd.1, bf16[256,256]{1,0:T(8,128)(2,1)} %qd.1, bf16[256,256]{1,0:T(8,128)(2,1)} %qwd.1, bf16[4,256,256]{2,1,0:T(8,128)(2,1)} %kvw.1, ...), custom_call_target="tpu_custom_call" | custom-call | tf_op jit(solution)/shard_map/pallas_call | solution.py:644
  187.1 1.9 copy.15

commit v6 on v5

--- a/solution.py
+++ b/solution.py
@@ -48,6 +48,7 @@
 class Ring:
     def __init__(self, n, buf, base, cuts, send, recv):
         self.n, self.buf, self.send, self.recv = n, buf, send, recv
+        self.base, self.cuts = base, cuts
         self.spans = []
         for cut in cuts:
             self.spans.append(pl.ds(base, cut))
@@ -64,29 +65,20 @@
 
     def piece(self, d, s, k, hops):
         ref = self.buf.at[self.origin(d, hops), self.spans[k if d == 0 else self.count - 1 - k]]
-        return remote(ref, ref, self.send.at[d, s, k], self.recv.at[d, s, k], self.to[d])
+        return remote(ref, ref, self.send.at[0], self.recv.at[s, k], self.to[d])
 
     def start(self, s, k):
         for d in (0, 1):
             self.piece(d, s, k, s).start()
 
     def land(self, s, k):
-        for d in (0, 1):
-            self.piece(d, s, k, s + 1).wait_recv()
+        both = pl.ds(self.base, self.cuts[k] + self.cuts[self.count - 1 - k])
+        ref = self.buf.at[self.me, both]
+        remote(ref, ref, self.send.at[0], self.recv.at[s, k], self.to[0]).wait_recv()
 
     def drain(self):
-        last = self.n // 2 - 1
-
-        def one(s, carry):
-            for k in range(self.count):
-                for d in (0, 1):
-                    self.piece(d, s, k, s).wait_send()
-            return carry
-
-        lax.fori_loop(0, last, one, 0)
-        for k in range(self.count // 2):
-            for d in (0, 1):
-                self.piece(d, last, k, last).wait_send()
+        ref = self.buf.at[pl.ds(0, self.n - 1), pl.ds(self.base, sum(self.cuts))]
+        remote(ref, ref, self.send.at[0], self.recv.at[0, 0], self.to[0]).wait_send()
 
 
 class Swap:
@@ -98,22 +90,22 @@
         self.kept = buf.shape[1] - cut
         self.base = pl.multiple_of(self.odd * cut, 16)
 
-    def piece(self, o, odd):
+    def piece(self, o, odd, sem):
         ref = self.buf.at[o, pl.ds(pl.multiple_of(odd * self.kept, 16), self.cut)]
-        return remote(ref, ref, self.send.at[o], self.recv.at[o], self.to)
-
-    def start(self, o):
-        self.piece(o, self.odd).start()
+        return remote(ref, ref, self.send.at[0], self.recv.at[sem], self.to)
+
+    def start(self, o, sem=None):
+        self.piece(o, self.odd, o if sem is None else sem).start()
 
     def land(self, o):
-        self.piece(o, 1 - self.odd).wait_recv()
+        self.piece(o, 1 - self.odd, o).wait_recv()
+
+    def several(self, count, sem):
+        ref = self.buf.at[pl.ds(0, count), pl.ds(0, self.cut)]
+        return remote(ref, ref, self.send.at[0], self.recv.at[sem], self.to)
 
     def drain(self):
-        def one(i, carry):
-            self.piece(lax.rem(lax.axis_index("sp") + i, self.n), self.odd).wait_send()
-            return carry
-
-        lax.fori_loop(1, self.n, one, 0)
+        self.several(self.n - 1, 0).wait_send()
 
 
 class Side:
@@ -144,18 +136,19 @@
         rel = 0 if k < 2 else (3 if d == 0 else 1)
         h = self.half_of(d, k)
         return remote(
-            self.source(rel, h), self.spot(rel, h, self.c), self.xs.at[d, k], self.xr.at[d, k], self.to[d]
+            self.source(rel, h), self.spot(rel, h, self.c), self.xs.at[0], self.xr.at[k], self.to[d]
         )
 
     def inward(self, d, k):
-        rel = (3 if d == 0 else 1) if k < 2 else 2
-        h = self.half_of(d, k)
-        ref = self.spot(rel, h, self.c)
-        return rel, h, remote(ref, ref, self.xs.at[d, k], self.xr.at[d, k], self.to[d])
+        return (3 if d == 0 else 1) if k < 2 else 2, self.half_of(d, k)
+
+    def blocks(self, count, send, recv, where):
+        ref = self.slots.at[pl.ds(0, count)]
+        return remote(ref, ref, send, recv, where)
 
     def across(self, rel, h):
         return remote(
-            self.source(rel, h), self.spot(rel, h, self.c), self.cs.at[rel, h], self.cr.at[rel, h], self.other
+            self.source(rel, h), self.spot(rel, h, self.c), self.cs.at[0], self.cr.at[0], self.other
         )
 
     def start(self):
@@ -166,30 +159,22 @@
             self.across(0, h).start()
 
     def step(self, k):
+        self.blocks(1, self.xs.at[0], self.xr.at[k], self.to[0]).wait_recv()
         for d in (0, 1):
-            rel, h, copy = self.inward(d, k)
-            copy.wait_recv()
             if k == 0:
                 self.out(d, 2).start()
-            self.across(rel, h).start()
+            self.across(*self.inward(d, k)).start()
 
     def finish(self):
-        for rel in range(NX):
-            for h in (0, 1):
-                ref = self.spot(rel, h, 1 - self.c)
-                remote(ref, ref, self.cs.at[rel, h], self.cr.at[rel, h], self.other).wait_recv()
+        self.blocks(NX, self.cs.at[0], self.cr.at[0], self.other).wait_recv()
 
     def drain(self):
-        for k in (0, 1, 2):
-            for d in (0, 1):
-                self.out(d, k).wait_send()
-        for rel in range(NX):
-            for h in (0, 1):
-                self.across(rel, h).wait_send()
+        self.blocks(NX - 1, self.xs.at[0], self.xr.at[0], self.to[0]).wait_send()
+        self.blocks(NX, self.cs.at[0], self.cr.at[0], self.other).wait_send()
 
 
 def side_sems():
-    return [DMA((2, 3)), DMA((2, 3)), DMA((NX, 2)), DMA((NX, 2))]
+    return [DMA((1,)), DMA((3,)), DMA((1,)), DMA((1,))]
 
 
 def layer_kernel(
@@ -268,9 +253,11 @@
         def one(j, carry):
             o = lax.rem(me + jnp.where(lax.rem(j, 2) == 1, (j + 1) // 2, n - j // 2), n)
 
-            @pl.when(j > 0)
-            def _():
-                swap.land(o)
+            if swap is not None:
+
+                @pl.when(j > 0)
+                def _():
+                    swap.land(o)
 
             total[...] += jnp.dot(nbuf[o], w[o], preferred_element_type=F32)
             return carry
@@ -283,13 +270,17 @@
         for d in (0, 1):
             swap.start(ring_.origin(d, hops))
 
+    def swap_late(hops):
+        for d in (0, 1):
+            swap2.start(ring2.origin(d, hops), jnp.where(2 * hops - d < n // 2, 0, 1))
+
     def hop2(s, k):
         ring2.land(s, k)
         ring2.start(s + 1, k)
 
     def late_swaps(lo, hi):
         def one(h, carry):
-            swap_both(swap2, ring2, h)
+            swap_late(h)
             return carry
 
         lax.fori_loop(lo, hi, one, 0)
@@ -356,7 +347,7 @@
     ring2.land(last - 1, 0)
     ring2.start(last, 0)
     ring2.land(last - 1, 1)
-    swap_both(swap2, ring2, last)
+    swap_late(last)
     gather(w1, swap1, acc1, n - 1, n)
     kvd = kbuf.shape[2]
     kbuf[me] = acc1[:, :kvd].astype(BF16)
@@ -376,12 +367,13 @@
         ref = kw.at[1 - c if inward else c, spans[i]]
         return remote(ref, ref, us.at[i], ur.at[i], side.other)
 
-    def trade(k, inward):
-        if inward:
-            ref = yd.at[2 * lax.rem(x + NX - k // 2, NX) + lax.rem(c + k % 2, 2)]
-            return remote(ref, ref, ts.at[k], tr.at[k], peer(k))
+    def trade(k):
         src = y.at[2 * lax.rem(x + k // 2, NX) + lax.rem(c + k % 2, 2)]
-        return remote(src, yd.at[t], ts.at[k], tr.at[k], peer(k))
+        return remote(src, yd.at[t], ts.at[0], tr.at[min(k - 1, 1)], peer(k))
+
+    def traded(count, sem):
+        ref = yd.at[pl.ds(0, count)]
+        return remote(ref, ref, ts.at[0], tr.at[sem], side.other)
 
     pass_on = remote(give, take, ws.at[0], wr.at[0], side.other)
 
@@ -488,7 +480,7 @@
                 @pl.when(s == 0)
                 def _():
                     ring2.land(last, 0)
-                    swap2.start(ring2.origin(0, last + 1))
+                    swap2.start(ring2.origin(0, last + 1), 1)
                     late.step(0)
 
                 @pl.when(s == 1)
@@ -497,7 +489,8 @@
 
                 @pl.when(s == 2)
                 def _():
-                    gather(w2, swap2, acc2, 0, n // 2)
+                    swap2.several(n // 2 - 1, 0).wait_recv()
+                    gather(w2, None, acc2, 0, n // 2)
 
                 @pl.when(s == 3)
                 def _():
@@ -506,22 +499,15 @@
 
                 @pl.when(s == 4)
                 def _():
-                    for i in (1, 2):
-                        twin(i, True).wait_recv()
-                    window(0, 2, rows // WINDOW - 1)
-
-                @pl.when(s == 5)
-                def _():
-                    pass_on.wait_recv()
-                    columns(to_sum)
-                    for d in (0, 1):
-                        relay(d, False).start()
+                    columns(to_give)
+                    pass_on.start()
 
             if k == 2:
 
                 @pl.when(s == 2)
                 def _():
-                    gather(w2, swap2, acc2, n // 2, n)
+                    swap2.several(n // 2, 1).wait_recv()
+                    gather(w2, None, acc2, n // 2, n)
                     kw[c, spans[0]] = acc2[:, wq:].astype(BF16)
                     qw[...] = acc2[:, :wq].astype(BF16)
                     for d in (0, 1):
@@ -537,8 +523,22 @@
 
                 @pl.when(s == 4)
                 def _():
-                    columns(to_give)
-                    pass_on.start()
+                    pass_on.wait_recv()
+                    columns(to_sum)
+                    for d in (0, 1):
+                        relay(d, False).start()
+
+                @pl.when(s == 5)
+                def _():
+                    merge()
+
+            if k == 3:
+
+                @pl.when(s == 3)
+                def _():
+                    for i in (1, 2):
+                        twin(i, True).wait_recv()
+                    window(0, 2, rows // WINDOW - 1)
 
             if k % 2 == 1:
 
@@ -553,8 +553,6 @@
         ring.land(last - 1, k)
         if k < 2:
             ring.start(last, k)
-        if k == 0:
-            merge()
         if k % 2 == 1:
             attend(ring.origin(k // 2, last - 1))
     late.finish()
@@ -585,7 +583,7 @@
     for k in (4, 5, 2, 6, 3, 7, 1):
         j = 2 * lax.rem(x + k // 2, NX) + lax.rem(c + k % 2, 2)
         y[j] = close(j)
-        trade(k, False).start()
+        trade(k).start()
     yd[t] = close(t)
     wide = 1024
 
@@ -613,13 +611,11 @@
 
     for d in (0, 1):
         deal(d, True).wait_recv()
-    trade(1, True).wait_recv()
+    traded(1, 0).wait_recv()
     lax.fori_loop(0, out.shape[1] // wide, begin, 0)
-    for k in range(2, 2 * NX):
-        trade(k, True).wait_recv()
+    traded(2 * NX - 2, 1).wait_recv()
     lax.fori_loop(0, out.shape[1] // wide, finish, 0)
-    for k in range(1, 2 * NX):
-        trade(k, False).wait_send()
+    traded(2 * NX - 1, 0).wait_send()
     for d in (0, 1):
         relay(d, False).wait_send()
         deal(d, False).wait_send()
@@ -675,14 +671,12 @@
             VMEM((block, model), F32),
             DMA((8,)),
         ]
-        + pair(2, hops, 4)
-        + pair(n)
-        + pair(2, hops, 2)
-        + pair(n)
-        + pair(2, hops, 4)
+        + [DMA((1,)), DMA((hops, 4)), DMA((1,)), DMA((n,))]
+        + [DMA((1,)), DMA((hops, 2)), DMA((1,)), DMA((2,))]
+        + [DMA((1,)), DMA((hops, 4))]
         + pair(2)
         + pair(3)
-        + pair(2 * NX)
+        + [DMA((1,)), DMA((2,))]
         + pair(5)
         + side_sems()
         + side_sems(),

time: 189 us -> 186 us (0.984)
  Pallas kernels: 186 us -> 183 us
    pallas_call x1, Pallas kernels: 186 us -> 183 us  [body(): pl.pallas_call(functools.partial(layer_kernel, n, sink.shape[0]), out_sha...]
where the time goes in v6:
time: 186 us
  Pallas kernels  183 us (98%)
  local copies, waits for them, and re-layouts  1.87 us (1%)
    pallas_call x1, Pallas kernels, body(): pl.pallas_call(functools.partial(layer_kernel, n, sink.shape[0]), out_sha...  183 us

profile of v6, /device:TPU:33, one launch (start us, length us, event | category | flops | bytes accessed | tf_op | source)
XLA Modules:
  0.0 185.9 jit_solution(3714357223315737164)
XLA Ops:
  0.7 183.4 %shard_map.118 = bf16[64,4096]{1,0:T(8,128)(2,1)} custom-call(bf16[64,4096]{1,0:T(8,128)(2,1)} %tok.1, f32[1,4096]{1,0:T(1,128)} %bitcast.2, bf16[256,256]{1,0:T(8,128)(2,1)} %kd.1, bf16[256,256]{1,0:T(8,128)(2,1)} %vd.1, bf16[256,256]{1,0:T(8,128)(2,1)} %qd.1, bf16[256,256]{1,0:T(8,128)(2,1)} %qwd.1, bf16[4,256,256]{2,1,0:T(8,128)(2,1)} %kvw.1, ...), custom_call_target="tpu_custom_call" | custom-call | tf_op jit(solution)/shard_map/pallas_call | solution.py:640
  184.0 1.9 %copy.15 = bf16[64,4096]{1,0:T(8,128)(2,1)} copy(bf16[64,4096]{1,0:T(8,128)(2,1)} %shard_map.118) | data formatting | bytes 1048576

commit v7 on v6

--- a/solution.py
+++ b/solution.py
@@ -14,7 +14,7 @@
 WINDOW = 128
 VDIM = 256
 NX = 4
-CUT = 96
+CUT = 80
 TP = ("tp_0", "tp_1")
 GRP_SP_TP = ("grp", "sp", "tp_0", "tp_1")
 EPS = 1e-06
@@ -208,7 +208,7 @@
 
     swap1 = Swap(n, w1, CUT, y1s, y1r)
     swap2 = Swap(n, w2, depth // 2, y2s, y2r)
-    ring1 = Ring(n, w1, swap1.base, (48, 32, 32, swap1.kept - 112), z1s, z1r)
+    ring1 = Ring(n, w1, swap1.base, (48, 48, 32, swap1.kept - 128), z1s, z1r)
     ring2 = Ring(n, w2, swap2.base, (depth // 4,) * 2, z2s, z2r)
     ring = Ring(n, kbuf, 0, (rows // 4,) * 4, zks, zkr)
     side = Side(None, raw, block // 2, *sems[:4])
@@ -285,6 +285,8 @@
 
         lax.fori_loop(lo, hi, one, 0)
 
+    done = 9
+
     def phase1(s, carry):
         for k in range(4):
             ring1.land(s, k)
@@ -308,17 +310,17 @@
 
             @pl.when(s == last - 2)
             def _():
-                gather(w1, swap1, acc1, 3 * k, min(3 * k + 3, 2 * last - 3))
+                gather(w1, swap1, acc1, (0, 3, 6, 8)[k], (3, 6, 8, done)[k])
 
             if k % 2 == 1:
 
-                @pl.when(s >= 2)
+                @pl.when(s == last - 2)
                 def _():
-                    hop2(s - 2, k // 2)
+                    hop2(0, k // 2)
 
         swap_both(swap1, ring1, s + 1)
 
-        @pl.when(s == 0)
+        @pl.when(s == last - 4)
         def _():
             for k in (0, 1):
                 ring2.start(0, k)
@@ -326,29 +328,25 @@
         return carry
 
     lax.fori_loop(0, last - 1, phase1, 0)
-    done = 2 * last - 3
     for k in range(4):
         ring1.land(last - 1, k)
         if k < 2:
             ring1.start(last, k)
         if k % 2 == 1:
-            hop2(last - 3, k // 2)
-        if k == 2:
-            gather(w1, swap1, acc1, done, done + 1)
+            hop2(1, k // 2)
     swap_both(swap1, ring1, last)
-    gather(w1, swap1, acc1, done + 1, done + 2)
+    gather(w1, swap1, acc1, done, done + 2)
     for k in (0, 1):
         ring1.land(last, k)
     swap1.start(ring1.origin(0, last + 1))
-    for k in (0, 1):
-        hop2(last - 2, k)
-    late_swaps(1, last)
-    gather(w1, swap1, acc1, done + 2, done + 4)
-    ring2.land(last - 1, 0)
-    ring2.start(last, 0)
-    ring2.land(last - 1, 1)
-    swap_late(last)
-    gather(w1, swap1, acc1, n - 1, n)
+    for s in (2, 3, 4):
+        for k in (0, 1):
+            hop2(s, k)
+        if s == 2:
+            late_swaps(1, s + 2)
+        else:
+            swap_late(s + 1)
+        gather(w1, swap1, acc1, done + 2 * s - 2, min(done + 2 * s, n))
     kvd = kbuf.shape[2]
     kbuf[me] = acc1[:, :kvd].astype(BF16)
     q[...] = acc1[:, kvd:].astype(BF16)
@@ -471,75 +469,97 @@
 
     attend(me)
 
+    def side_work(s, k):
+        def at(when):
+            return pl.when(s == when)
+
+        if k == 0:
+
+            @at(0)
+            def _():
+                for i in (0, 1):
+                    hop2(last - 2, i)
+                swap_late(last - 1)
+
+            @at(1)
+            def _():
+                ring2.land(last - 1, 0)
+                ring2.start(last, 0)
+                ring2.land(last - 1, 1)
+                swap_late(last)
+
+            @at(4)
+            def _():
+                late.step(2)
+
+        if k == 1:
+
+            @at(1)
+            def _():
+                late.step(1)
+
+            @at(3)
+            def _():
+                swap2.several(n // 2, 1).wait_recv()
+                gather(w2, None, acc2, n // 2, n)
+                kw[c, spans[0]] = acc2[:, wq:].astype(BF16)
+                qw[...] = acc2[:, :wq].astype(BF16)
+                for d in (0, 1):
+                    edge(d, False).start()
+                twin(0, False).start()
+
+            @at(4)
+            def _():
+                for d in (0, 1):
+                    edge(d, True).wait_recv()
+                    twin(d + 1, False).start()
+
+            @at(5)
+            def _():
+                pass_on.wait_recv()
+                columns(to_sum)
+                for d in (0, 1):
+                    relay(d, False).start()
+
+        if k == 2:
+
+            @at(0)
+            def _():
+                late.step(0)
+
+            @at(1)
+            def _():
+                ring2.land(last, 0)
+                swap2.start(ring2.origin(0, last + 1), 1)
+
+            @at(2)
+            def _():
+                swap2.several(n // 2 - 1, 0).wait_recv()
+                gather(w2, None, acc2, 0, n // 2)
+
+            @at(3)
+            def _():
+                twin(0, True).wait_recv()
+                window(1, rows // WINDOW - 1, 1)
+
+            @at(4)
+            def _():
+                for i in (1, 2):
+                    twin(i, True).wait_recv()
+                window(0, 2, rows // WINDOW - 1)
+
+        if k == 3:
+
+            @at(4)
+            def _():
+                columns(to_give)
+                pass_on.start()
+
     def phase2(s, carry):
         for k in range(4):
             ring.land(s, k)
             ring.start(s + 1, k)
-            if k == 0:
-
-                @pl.when(s == 0)
-                def _():
-                    ring2.land(last, 0)
-                    swap2.start(ring2.origin(0, last + 1), 1)
-                    late.step(0)
-
-                @pl.when(s == 1)
-                def _():
-                    late.step(1)
-
-                @pl.when(s == 2)
-                def _():
-                    swap2.several(n // 2 - 1, 0).wait_recv()
-                    gather(w2, None, acc2, 0, n // 2)
-
-                @pl.when(s == 3)
-                def _():
-                    twin(0, True).wait_recv()
-                    window(1, rows // WINDOW - 1, 1)
-
-                @pl.when(s == 4)
-                def _():
-                    columns(to_give)
-                    pass_on.start()
-
-            if k == 2:
-
-                @pl.when(s == 2)
-                def _():
-                    swap2.several(n // 2, 1).wait_recv()
-                    gather(w2, None, acc2, n // 2, n)
-                    kw[c, spans[0]] = acc2[:, wq:].astype(BF16)
-                    qw[...] = acc2[:, :wq].astype(BF16)
-                    for d in (0, 1):
-                        edge(d, False).start()
-                    twin(0, False).start()
-
-                @pl.when(s == 3)
-                def _():
-                    for d in (0, 1):
-                        edge(d, True).wait_recv()
-                        twin(d + 1, False).start()
-                    late.step(2)
-
-                @pl.when(s == 4)
-                def _():
-                    pass_on.wait_recv()
-                    columns(to_sum)
-                    for d in (0, 1):
-                        relay(d, False).start()
-
-                @pl.when(s == 5)
-                def _():
-                    merge()
-
-            if k == 3:
-
-                @pl.when(s == 3)
-                def _():
-                    for i in (1, 2):
-                        twin(i, True).wait_recv()
-                    window(0, 2, rows // WINDOW - 1)
-
+            side_work(s, k)
             if k % 2 == 1:
 
                 @pl.when(s > 0)
@@ -553,6 +573,8 @@
         ring.land(last - 1, k)
         if k < 2:
             ring.start(last, k)
+        if k == 1:
+            merge()
         if k % 2 == 1:
             attend(ring.origin(k // 2, last - 1))
     late.finish()

time: 186 us -> 190 us (1.022)
  Pallas kernels: 183 us -> 187 us
    pallas_call x1, Pallas kernels: 183 us -> 187 us  [body(): pl.pallas_call(functools.partial(layer_kernel, n, sink.shape[0]), out_sha...]
where the time goes in v7:
time: 190 us; the launch traced here: 189 us
  Pallas kernels  187 us (98%)
    pallas_call x1, Pallas kernels, body(): pl.pallas_call(functools.partial(layer_kernel, n, sink.shape[0]), out_sha...  187 us

profile of v7, /device:TPU:33, one launch (start us, length us, event | category | flops | bytes accessed | tf_op | source)
XLA Modules:
  0.0 189.3 jit_solution(7383267640004227918)
XLA Ops:
  0.7 186.8 %shard_map.118 = bf16[64,4096]{1,0:T(8,128)(2,1)} custom-call(bf16[64,4096]{1,0:T(8,128)(2,1)} %tok.1, f32[1,4096]{1,0:T(1,128)} %bitcast.2, bf16[256,256]{1,0:T(8,128)(2,1)} %kd.1, bf16[256,256]{1,0:T(8,128)(2,1)} %vd.1, bf16[256,256]{1,0:T(8,128)(2,1)} %qd.1, bf16[256,256]{1,0:T(8,128)(2,1)} %qwd.1, bf16[4,256,256]{2,1,0:T(8,128)(2,1)} %kvw.1, ...), custom_call_target="tpu_custom_call" | custom-call | tf_op jit(solution)/shard_map/pallas_call | solution.py:662
  187.4 1.9 copy.15

commit v8 on v7

--- a/solution.py
+++ b/solution.py
@@ -14,7 +14,7 @@
 WINDOW = 128
 VDIM = 256
 NX = 4
-CUT = 80
+CUT = 96
 TP = ("tp_0", "tp_1")
 GRP_SP_TP = ("grp", "sp", "tp_0", "tp_1")
 EPS = 1e-06
@@ -208,7 +208,7 @@
 
     swap1 = Swap(n, w1, CUT, y1s, y1r)
     swap2 = Swap(n, w2, depth // 2, y2s, y2r)
-    ring1 = Ring(n, w1, swap1.base, (48, 48, 32, swap1.kept - 128), z1s, z1r)
+    ring1 = Ring(n, w1, swap1.base, (48, 32, 32, swap1.kept - 112), z1s, z1r)
     ring2 = Ring(n, w2, swap2.base, (depth // 4,) * 2, z2s, z2r)
     ring = Ring(n, kbuf, 0, (rows // 4,) * 4, zks, zkr)
     side = Side(None, raw, block // 2, *sems[:4])
@@ -285,7 +285,7 @@
 
         lax.fori_loop(lo, hi, one, 0)
 
-    done = 9
+    done = 2 * last - 3
 
     def phase1(s, carry):
         for k in range(4):
@@ -310,17 +310,17 @@
 
             @pl.when(s == last - 2)
             def _():
-                gather(w1, swap1, acc1, (0, 3, 6, 8)[k], (3, 6, 8, done)[k])
+                gather(w1, swap1, acc1, 3 * k, min(3 * k + 3, done))
 
             if k % 2 == 1:
 
-                @pl.when(s == last - 2)
+                @pl.when(s >= 3)
                 def _():
-                    hop2(0, k // 2)
+                    hop2(s - 3, k // 2)
 
         swap_both(swap1, ring1, s + 1)
 
-        @pl.when(s == last - 4)
+        @pl.when(s == 1)
         def _():
             for k in (0, 1):
                 ring2.start(0, k)
@@ -333,20 +333,19 @@
         if k < 2:
             ring1.start(last, k)
         if k % 2 == 1:
-            hop2(1, k // 2)
+            hop2(last - 4, k // 2)
     swap_both(swap1, ring1, last)
-    gather(w1, swap1, acc1, done, done + 2)
     for k in (0, 1):
         ring1.land(last, k)
     swap1.start(ring1.origin(0, last + 1))
-    for s in (2, 3, 4):
-        for k in (0, 1):
-            hop2(s, k)
-        if s == 2:
-            late_swaps(1, s + 2)
-        else:
-            swap_late(s + 1)
-        gather(w1, swap1, acc1, done + 2 * s - 2, min(done + 2 * s, n))
+    for k in (0, 1):
+        hop2(last - 3, k)
+    late_swaps(1, last - 1)
+    gather(w1, swap1, acc1, done, done + 2)
+    for k in (0, 1):
+        hop2(last - 2, k)
+    swap_late(last - 1)
+    gather(w1, swap1, acc1, done + 2, n)
     kvd = kbuf.shape[2]
     kbuf[me] = acc1[:, :kvd].astype(BF16)
     q[...] = acc1[:, kvd:].astype(BF16)
@@ -477,20 +476,21 @@
 
             @at(0)
             def _():
-                for i in (0, 1):
-                    hop2(last - 2, i)
-                swap_late(last - 1)
-
-            @at(1)
-            def _():
                 ring2.land(last - 1, 0)
                 ring2.start(last, 0)
                 ring2.land(last - 1, 1)
                 swap_late(last)
 
+            @at(1)
+            def _():
+                ring2.land(last, 0)
+                swap2.start(ring2.origin(0, last + 1), 1)
+
             @at(4)
             def _():
-                late.step(2)
+                for i in (1, 2):
+                    twin(i, True).wait_recv()
+                window(0, 2, rows // WINDOW - 1)
 
         if k == 1:
 
@@ -498,7 +498,30 @@
             def _():
                 late.step(1)
 
+            @at(2)
+            def _():
+                swap2.several(n // 2 - 1, 0).wait_recv()
+                gather(w2, None, acc2, 0, n // 2)
+
             @at(3)
+            def _():
+                twin(0, True).wait_recv()
+                window(1, rows // WINDOW - 1, 1)
+
+            @at(4)
+            def _():
+                columns(to_give)
+                pass_on.start()
+
+        if k == 2:
+
+            @at(0)
+            def _():
+                late.step(0)
+
+        if k == 3:
+
+            @at(2)
             def _():
                 swap2.several(n // 2, 1).wait_recv()
                 gather(w2, None, acc2, n // 2, n)
@@ -508,52 +531,23 @@
                     edge(d, False).start()
                 twin(0, False).start()
 
-            @at(4)
+            @at(3)
             def _():
                 for d in (0, 1):
                     edge(d, True).wait_recv()
                     twin(d + 1, False).start()
-
-            @at(5)
+                late.step(2)
+
+            @at(4)
             def _():
                 pass_on.wait_recv()
                 columns(to_sum)
                 for d in (0, 1):
                     relay(d, False).start()
 
-        if k == 2:
-
-            @at(0)
-            def _():
-                late.step(0)
-
-            @at(1)
-            def _():
-                ring2.land(last, 0)
-                swap2.start(ring2.origin(0, last + 1), 1)
-
-            @at(2)
-            def _():
-                swap2.several(n // 2 - 1, 0).wait_recv()
-                gather(w2, None, acc2, 0, n // 2)
-
-            @at(3)
-            def _():
-                twin(0, True).wait_recv()
-                window(1, rows // WINDOW - 1, 1)
-
-            @at(4)
-            def _():
-                for i in (1, 2):
-                    twin(i, True).wait_recv()
-                window(0, 2, rows // WINDOW - 1)
-
-        if k == 3:
-
-            @at(4)
-            def _():
-                columns(to_give)
-                pass_on.start()
+            @at(5)
+            def _():
+                merge()
 
     def phase2(s, carry):
         for k in range(4):
@@ -573,8 +567,6 @@
         ring.land(last - 1, k)
         if k < 2:
             ring.start(last, k)
-        if k == 1:
-            merge()
         if k % 2 == 1:
             attend(ring.origin(k // 2, last - 1))
     late.finish()

time: 190 us -> 186 us (0.979)
  Pallas kernels: 187 us -> 183 us
    pallas_call x1, Pallas kernels: 187 us -> 183 us  [body(): pl.pallas_call(functools.partial(layer_kernel, n, sink.shape[0]), out_sha...]
where the time goes in v8:
time: 186 us
  Pallas kernels  183 us (98%)
  local copies, waits for them, and re-layouts  1.87 us (1%)
    pallas_call x1, Pallas kernels, body(): pl.pallas_call(functools.partial(layer_kernel, n, sink.shape[0]), out_sha...  183 us

profile of v8, /device:TPU:33, one launch (start us, length us, event | category | flops | bytes accessed | tf_op | source)
XLA Modules:
  0.0 185.6 jit_solution(7163976529181167157)
XLA Ops:
  0.7 183.1 %shard_map.118 = bf16[64,4096]{1,0:T(8,128)(2,1)} custom-call(bf16[64,4096]{1,0:T(8,128)(2,1)} %tok.1, f32[1,4096]{1,0:T(1,128)} %bitcast.2, bf16[256,256]{1,0:T(8,128)(2,1)} %kd.1, bf16[256,256]{1,0:T(8,128)(2,1)} %vd.1, bf16[256,256]{1,0:T(8,128)(2,1)} %qd.1, bf16[256,256]{1,0:T(8,128)(2,1)} %qwd.1, bf16[4,256,256]{2,1,0:T(8,128)(2,1)} %kvw.1, ...), custom_call_target="tpu_custom_call" | custom-call | tf_op jit(solution)/shard_map/pallas_call | solution.py:654
  183.7 1.9 %copy.15 = bf16[64,4096]{1,0:T(8,128)(2,1)} copy(bf16[64,4096]{1,0:T(8,128)(2,1)} %shard_map.118) | data formatting | bytes 1048576

commit v9 on v8

--- a/solution.py
+++ b/solution.py
@@ -599,7 +599,7 @@
         y[j] = close(j)
         trade(k).start()
     yd[t] = close(t)
-    wide = 1024
+    wide = 2048
 
     def add(total, away, cols):
         first = 2 * lax.rem(x + NX - away, NX)

time: 186 us -> 186 us (level)
  no operation moved by 1% of the time
where the time goes in v9:
time: 186 us; the launch traced here: 185 us
  Pallas kernels  183 us (98%)
  local copies, waits for them, and re-layouts  1.87 us (1%)
    pallas_call x1, Pallas kernels, body(): pl.pallas_call(functools.partial(layer_kernel, n, sink.shape[0]), out_sha...  183 us

profile of v9, /device:TPU:33, one launch (start us, length us, event | category | flops | bytes accessed | tf_op | source)
XLA Modules:
  0.0 185.3 jit_solution(17646647440610571986)
XLA Ops:
  0.7 182.8 %shard_map.118 = bf16[64,4096]{1,0:T(8,128)(2,1)} custom-call(bf16[64,4096]{1,0:T(8,128)(2,1)} %tok.1, f32[1,4096]{1,0:T(1,128)} %bitcast.2, bf16[256,256]{1,0:T(8,128)(2,1)} %kd.1, bf16[256,256]{1,0:T(8,128)(2,1)} %vd.1, bf16[256,256]{1,0:T(8,128)(2,1)} %qd.1, bf16[256,256]{1,0:T(8,128)(2,1)} %qwd.1, bf16[4,256,256]{2,1,0:T(8,128)(2,1)} %kvw.1, ...), custom_call_target="tpu_custom_call" | custom-call | tf_op jit(solution)/shard_map/pallas_call | solution.py:654
  183.5 1.9 %copy.15 = bf16[64,4096]{1,0:T(8,128)(2,1)} copy(bf16[64,4096]{1,0:T(8,128)(2,1)} %shard_map.118) | data formatting | bytes 1048576
